TPU v7x, 512 devices: a whole 4x4x16 slice. The times are simulated.
512 devices in a mesh: ep: 128 (over z, x, core), tp: 4 (over y).
Axes of the slice: x: 4, y: 4, z: 16, core: 2. Of those that a mesh axis runs over, the one named last changes fastest.
Arguments:
- hidden: bfloat16 [512, 2048], P('ep'), may hold values from -6 to 6
- attn_gain: float32 [2048], replicated, may hold values from 0.3 to 3
- query_weight: bfloat16 [2048, 2048], P('ep', 'tp'), may hold values from -0.125 to 0.125
- head_bias: float32 [16], replicated, may hold values from -10 to -4
- key_cache: bfloat16 [512, 4, 1024, 128], P('ep', 'tp'), may hold values from -6 to 6
- value_cache: bfloat16 [512, 4, 1024, 128], P('ep', 'tp'), may hold values from -7 to 7
- lengths: int32 [512], P('ep'), may hold values from 256 to 1024, as said below
- out_weight: bfloat16 [2048, 2048], P('tp', 'ep'), may hold values from -0.125 to 0.125
- moe_gain: float32 [2048], replicated, may hold values from 0.1 to 1.9
- route_group: int32 [512], P('ep'), may hold values from 0 to 3, as said below
- route_inner: int32 [512, 2], P('ep'), may hold values from 0 to 31, as said below
- route_weight: bfloat16 [512, 2], P('ep'), may hold values from 0.25 to 1
- gate_w: bfloat16 [128, 2048, 768], P('ep', None, 'tp'), may hold values from -0.125 to 0.125
- up_w: bfloat16 [128, 2048, 768], P('ep', None, 'tp'), may hold values from -0.125 to 0.125
- down_w: bfloat16 [128, 768, 2048], P('ep', 'tp'), may hold values from -0.21875 to 0.21875
Outputs:
- mixed: bfloat16 [512, 2048], P('ep', 'tp')
Inputs may be any that keep to these rules, and one draw needn't show every extreme that they name: `lengths`: some sequence has length 1024 in every draw. Within the rows of one device (aligned blocks of 4 rows) no expert route_group * 32 + route_inner is named twice; one expert is named in every block. `route_inner`: the 2 entries of a row differ.
All inputs are finite; a program needn't handle non-finite values.
Results may differ from a plain program's by a relative error of at most 0.013.
Values may be sent and summed in bfloat16 or wider, within the bound.
A program may use at most 64 MiB of HBM per device.

v0:
```python
import jax
import jax.numpy as jnp
from jax import lax
from jax.sharding import Mesh
from jax.sharding import PartitionSpec as P

EP = ("ep_0", "ep_1", "ep_2")


rms_epsilon = 1e-06


def joined_along(tiles, dim):
    lengths = list(tiles.shape[1:])
    lengths[dim] *= tiles.shape[0]
    return jnp.moveaxis(tiles, 0, dim).reshape(lengths)


def gather_in_order(shard, axes, sequence):
    tiles = shard[None]
    for k in sequence:
        tiles = lax.all_gather(tiles, axes[k], axis=0, tiled=True)
    current = [lax.axis_size(axes[k]) for k in reversed(sequence)]
    tiles = tiles.reshape(*current, *shard.shape)
    turned = sorted(range(len(sequence)), key=lambda place: sequence[len(sequence) - 1 - place])
    return tiles.transpose(*turned, *range(len(sequence), tiles.ndim)).reshape(-1, *shard.shape)


def gathered_by_axis(shard, axes, sequence, dim):
    return joined_along(gather_in_order(shard, axes, sequence), dim)


def in_blocks(shard, dim, peers):
    lengths = shard.shape
    tiles = shard.reshape(*lengths[:dim], peers, lengths[dim] // peers, *lengths[dim + 1 :])
    return jnp.moveaxis(tiles, dim, 0)


def moved_by_axis(tiles, axes, sequence):
    lengths = [lax.axis_size(a) for a in axes]
    tiles = tiles.reshape(*lengths, *tiles.shape[1:])
    for k in sequence:
        tiles = lax.all_to_all(tiles, axes[k], split_axis=k, concat_axis=k, tiled=True)
    return tiles.reshape(-1, *tiles.shape[len(axes) :])


def core_and_chips(shard, groups, sequence, split_dim, concat_dim):
    peers = lax.axis_size(groups[0]) * lax.axis_size(groups[1])
    tiles = in_blocks(shard, split_dim, peers)
    return joined_along(moved_by_axis(tiles, groups, sequence), concat_dim)


def sum_at_owner(shard, axis, dim):
    peers = lax.axis_size(axis)
    tiles = lax.all_to_all(in_blocks(shard, dim, peers), axis, 0, 0, tiled=True)
    return jnp.sum(tiles.astype(jnp.float32), axis=0)


def rms_scale(values, gain):
    wide = values.astype(jnp.float32)
    scaled = wide * lax.rsqrt(jnp.mean(wide * wide, axis=-1, keepdims=True) + rms_epsilon)
    return (scaled * gain).astype(jnp.bfloat16)


def body(
    hidden,
    attn_gain,
    query_weight,
    head_bias,
    key_cache,
    value_cache,
    lengths,
    out_weight,
    moe_gain,
    route_group,
    route_inner,
    route_weight,
    gate_w,
    up_w,
    down_w,
):
    n_tp = lax.axis_size("tp")
    n_ep = lax.axis_size(EP)
    tokens = hidden.shape[0]
    d_model = hidden.shape[1]
    normed = rms_scale(hidden, attn_gain)
    queries = jnp.dot(
        normed, gathered_by_axis(query_weight, EP, (1, 0, 2), 0), preferred_element_type=jnp.float32
    ).astype(jnp.bfloat16)
    head_size = key_cache.shape[3]
    local_kv = key_cache.shape[1]
    cache_len = key_cache.shape[2]
    local_heads = queries.shape[1] // head_size
    group_heads = local_heads // local_kv
    queries = queries.reshape(tokens, local_kv, group_heads, head_size)
    own_bias = lax.dynamic_slice_in_dim(
        head_bias, lax.axis_index("tp") * local_heads, local_heads, 0
    )
    own_bias = own_bias.reshape(local_kv, group_heads)
    scores = jnp.einsum(
        "tkgd,tkpd->tkgp", queries, key_cache, preferred_element_type=jnp.float32
    ) * head_size ** (-0.5)
    scores = scores + own_bias[None, :, :, None]
    position = jnp.arange(cache_len, dtype=jnp.int32)
    visible = position[None, None, None, :] < lengths[:, None, None, None]
    log_keep = jnp.where(visible, jax.nn.log_sigmoid(-scores), 0.0)
    later_sum = lax.cumsum(log_keep, axis=3, reverse=True) - log_keep
    weight = jnp.where(visible, jnp.exp(jax.nn.log_sigmoid(scores) + later_sum), 0.0).astype(
        jnp.bfloat16
    )
    heads_out = jnp.einsum(
        "tkgp,tkpd->tkgd", weight, value_cache, preferred_element_type=jnp.float32
    )
    heads_out = heads_out.astype(jnp.bfloat16).reshape(tokens, -1)
    partial_value = jnp.dot(
        gathered_by_axis(heads_out, EP, (1, 0, 2), 0),
        out_weight,
        preferred_element_type=jnp.float32,
    )
    rounded = lax.optimization_barrier(partial_value.astype(jnp.bfloat16)).astype(jnp.float32)
    col_total = lax.psum(rounded.astype(jnp.bfloat16), "tp").astype(jnp.float32)
    attended = lax.all_to_all(
        col_total.astype(jnp.bfloat16), EP, split_axis=0, concat_axis=1, tiled=True
    ).astype(col_total.dtype)
    residual = (hidden.astype(jnp.float32) + attended).astype(jnp.bfloat16)
    normed_two = rms_scale(residual, moe_gain)
    per_device = gate_w.shape[0]
    experts = per_device * n_ep
    group_count = max(2, experts // 32)
    group_size = experts // group_count
    chosen = route_group[:, None] * group_size + route_inner
    matches = chosen[:, :, None] == jnp.arange(experts, dtype=jnp.int32)[None, None, :]
    picked = jnp.any(matches, axis=1).astype(jnp.bfloat16)
    mixing = jnp.sum(
        jnp.where(matches, route_weight[:, :, None].astype(jnp.float32), 0.0), axis=1
    ).astype(jnp.bfloat16)
    part_width = d_model // n_tp
    own_cols = lax.dynamic_slice_in_dim(
        normed_two, lax.axis_index("tp") * part_width, part_width, 1
    )
    outgoing = jnp.einsum("te,td->ed", picked, own_cols, preferred_element_type=jnp.float32)
    outgoing = outgoing.astype(jnp.bfloat16).reshape(n_ep, per_device, part_width)
    arrived = core_and_chips(outgoing, (("ep_0", "ep_1"), "ep_2"), (1, 0), 0, 0)
    arrived = lax.all_gather(arrived, "tp", axis=2, tiled=True)
    gated_in = jnp.einsum("sed,edf->sef", arrived, gate_w, preferred_element_type=jnp.float32)
    up_proj = jnp.einsum("sed,edf->sef", arrived, up_w, preferred_element_type=jnp.float32)
    activated = (jax.nn.silu(gated_in) * up_proj).astype(jnp.bfloat16)
    down_out = jnp.einsum("sef,efd->sed", activated, down_w, preferred_element_type=jnp.float32)
    down_rounded = lax.optimization_barrier(down_out.astype(jnp.bfloat16)).astype(jnp.float32)
    summed = sum_at_owner(down_rounded.astype(jnp.bfloat16), "tp", 2).astype(jnp.bfloat16)
    returned = lax.all_to_all(summed, EP, split_axis=0, concat_axis=0, tiled=True).reshape(
        experts, part_width
    )
    routed = jnp.dot(mixing, returned, preferred_element_type=jnp.float32)
    own_residual = lax.dynamic_slice_in_dim(
        residual, lax.axis_index("tp") * part_width, part_width, 1
    )
    return (own_residual.astype(jnp.float32) + routed).astype(jnp.bfloat16)


def solution(mesh):
    torus = Mesh(mesh.devices.reshape(16, 4, 2, mesh.shape["tp"]), ("ep_0", "ep_1", "ep_2", "tp"))
    placed = (
        P(EP, None),
        P(),
        P(EP, "tp"),
        P(),
        P(EP, "tp", None, None),
        P(EP, "tp", None, None),
        P(EP),
        P("tp", EP),
        P(),
        P(EP),
        P(EP, None),
        P(EP, None),
        P(EP, None, "tp"),
        P(EP, None, "tp"),
        P(EP, "tp", None),
    )
    return jax.shard_map(body, mesh=torus, in_specs=placed, out_specs=P(EP, "tp"), check_vma=False)
```

profile of v0, /device:TPU:1, one launch (start us, length us, event | category | flops | bytes accessed | tf_op | source)
XLA Modules:
  0.0 320.1 jit_solution(2171377821161092385)
XLA Ops:
  6.5 12.0 %all-gather = bf16[64,512]{1,0:T(8,128)(2,1)} all-gather(bf16[16,512]{1,0:T(8,128)(2,1)} %param.17), channel_id=2, replica_groups=mesh['ep_0'=16,'ep_1'=4,'ep_2'=2,'tp'=4] {'ep_1'}, dimensions={0}, use_global_device_ids=true | all-gather | bytes 81920 | tf_op jit(solution)/shard_map/all_gather | solution.py:22
  18.6 66.4 %all-gather.4.cloned.1.call-done = bf16[64,16,512]{2,1,0:T(8,128)(2,1)} async-done(((bf16[4,16,512]{2,1,0:T(8,128)(2,1)}), bf16[64,16,512]{2,1,0:T(8,128)(2,1)}) %all-gather.4.cloned.1.call-update) | async-done | bytes 1048592 | tf_op jit(solution)/shard_map/all_gather | solution.py:22
  85.0 0.7 dynamic_slice.9
  85.8 0.8 dynamic-slice
  86.5 0.8 fusion.31
  87.4 0.7 broadcast_multiply_fusion
  88.1 0.7 broadcast_add_fusion
  88.7 0.7 iota_compare_fusion
  89.5 27.5 %all-gather.6.cloned.1.call-done = bf16[128,16,512]{2,1,0:T(8,128)(2,1)} async-done(((bf16[64,16,512]{2,1,0:T(8,128)(2,1)}), bf16[128,16,512]{2,1,0:T(8,128)(2,1)}) %all-gather.6.cloned.1.call-update) | async-done | bytes 2097168 | tf_op jit(solution)/shard_map/all_gather | solution.py:22
  117.0 1.8 copy.53
  118.8 0.4 convolution_convert_fusion.4
  119.3 0.4 fusion.29
  119.7 19.8 %reduce-window.6 = f32[4,1,4,8,128]{4,3,2,1,0:T(8,128)S(1)} reduce-window(f32[4,1,4,8,128]{4,3,2,1,0:T(8,128)S(1)} %bitcast.101, f32[]{:T(128)} %constant.9.clone.1), window={size=1x1x1x1x128 pad=0_0x0_0x0_0x0_0x0_127}, to_apply=%region_1.2 | reduce-window | flops 2080768 | bytes 131076 | tf_op jit(solution)/shard_map/reduce-window
  139.7 0.7 reduce-window.9
  141.0 9.1 %all_gather.24 = bf16[4,4,512]{2,1,0:T(4,128)(2,1)S(1)} all-gather(bf16[1,4,512]{2,1,0:T(4,128)(2,1)S(1)} %broadcast_in_dim_reshape.4), channel_id=1, replica_groups=mesh['ep_0'=16,'ep_1'=4,'ep_2'=2,'tp'=4] {'ep_1'}, dimensions={0}, use_global_device_ids=true | all-gather | bytes 20480 | tf_op jit(solution)/shard_map/all_gather | solution.py:22
  150.1 24.1 %all_gather.25 = bf16[64,4,512]{2,1,0:T(4,128)(2,1)S(1)} all-gather(bf16[4,4,512]{2,1,0:T(4,128)(2,1)S(1)} %all_gather.24), channel_id=1, replica_groups=mesh['ep_0'=16,'ep_1'=4,'ep_2'=2,'tp'=4] {'ep_0'}, dimensions={0}, use_global_device_ids=true | all-gather | bytes 278528 | tf_op jit(solution)/shard_map/all_gather | solution.py:22
  174.2 11.7 %all_gather.26 = bf16[128,4,512]{2,1,0:T(4,128)(2,1)S(1)} all-gather(bf16[64,4,512]{2,1,0:T(4,128)(2,1)S(1)} %all_gather.25), channel_id=1, replica_groups=mesh['ep_0'=16,'ep_1'=4,'ep_2'=2,'tp'=4] {'ep_2'}, dimensions={0}, use_global_device_ids=true | all-gather | bytes 786432 | tf_op jit(solution)/shard_map/all_gather | solution.py:22
  186.6 15.2 %psum.7 = bf16[128,4,16]{2,1,0:T(4,128)(2,1)} all-reduce(bf16[128,4,16]{2,1,0:T(4,128)(2,1)S(1)} %bitcast.98), channel_id=1, replica_groups=mesh['ep_0'=16,'ep_1'=4,'ep_2'=2,'tp'=4] {'tp'}, use_global_device_ids=true, to_apply=%region_3.4 | all-reduce | flops 8192 | bytes 32768 | tf_op jit(solution)/shard_map/psum | solution.py:121
  201.8 15.9 %all-to-all-start = ((bf16[128,4,16]{2,1,0:T(4,128)(2,1)}), bf16[128,4,16]{2,1,0:T(4,128)(2,1)S(1)}, u32[]{:S(2)}, u32[]{:S(2)}) async-start(bf16[128,4,16]{2,1,0:T(4,128)(2,1)} %psum.7), calls=%async_computation | async-start | bytes 262144 | tf_op jit(solution)/shard_map/all_to_all | solution.py:122
  217.9 15.9 %all-to-all-done = bf16[128,4,16]{2,1,0:T(4,128)(2,1)S(1)} async-done(((bf16[128,4,16]{2,1,0:T(4,128)(2,1)}), bf16[128,4,16]{2,1,0:T(4,128)(2,1)S(1)}, u32[]{:S(2)}, u32[]{:S(2)}) %all-to-all-start) | async-done | bytes 16416 | tf_op jit(solution)/shard_map/all_to_all | solution.py:122
  234.5 3.9 %all_to_all.33 = bf16[64,2,1,1,512]{4,0,3,2,1:T(8,128)(2,1)S(1)} all-to-all(bf16[64,2,1,1,512]{4,0,3,2,1:T(8,128)(2,1)S(1)} %copy.58), channel_id=1, replica_groups=mesh['ep_0'=16,'ep_1'=4,'ep_2'=2,'tp'=4] {'ep_2'}, dimensions={1} | all-to-all | bytes 262144 | tf_op jit(solution)/shard_map/all_to_all | solution.py:43
  238.5 21.2 %all_to_all.34 = bf16[64,2,1,1,512]{4,1,3,2,0:T(2,128)(2,1)S(1)} all-to-all(bf16[64,2,1,1,512]{4,1,3,2,0:T(2,128)(2,1)S(1)} %copy.59), channel_id=1, replica_groups=mesh['ep_0'=16,'ep_1'=4,'ep_2'=2,'tp'=4] {'ep_0','ep_1'}, dimensions={0} | all-to-all | bytes 262144 | tf_op jit(solution)/shard_map/all_to_all | solution.py:43
  259.8 11.2 %all_gather.27 = bf16[128,1,2048]{2,0,1:T(8,128)(2,1)S(1)} all-gather(bf16[128,1,512]{2,0,1:T(8,128)(2,1)S(1)} %reshape_reshape.11), channel_id=1, replica_groups=mesh['ep_0'=16,'ep_1'=4,'ep_2'=2,'tp'=4] {'tp'}, dimensions={2}, use_global_device_ids=true | all-gather | bytes 655360 | tf_op jit(solution)/shard_map/all_gather | solution.py:144
  271.0 0.4 convolution_bitcast_fusion.1
  271.4 2.1 fusion
  273.5 9.3 %all_to_all.35 = bf16[4,128,1,512]{3,1,2,0:T(8,128)(2,1)S(1)} all-to-all(bf16[4,128,1,512]{3,1,2,0:T(8,128)(2,1)S(1)} %bitcast.96), channel_id=1, replica_groups=mesh['ep_0'=16,'ep_1'=4,'ep_2'=2,'tp'=4] {'tp'}, dimensions={0} | all-to-all | bytes 1048576 | tf_op jit(solution)/shard_map/all_to_all | solution.py:55
  282.9 0.5 broadcast.80
  283.4 0.7 reduce.4
  284.1 0.7 reshape.171
  284.8 11.4 %all-to-all-start.4 = ((bf16[128,2,256]{2,1,0:T(2,128)(2,1)}), bf16[128,2,256]{2,1,0:T(2,128)(2,1)S(1)}, u32[]{:S(2)}, u32[]{:S(2)}) async-start(bf16[128,2,256]{2,1,0:T(2,128)(2,1)} %reshape.171), calls=%async_computation.4 | async-start | bytes 262144 | tf_op jit(solution)/shard_map/all_to_all | solution.py:151
  296.3 16.1 %all-to-all-done.4 = bf16[128,2,256]{2,1,0:T(2,128)(2,1)S(1)} async-done(((bf16[128,2,256]{2,1,0:T(2,128)(2,1)}), bf16[128,2,256]{2,1,0:T(2,128)(2,1)S(1)}, u32[]{:S(2)}, u32[]{:S(2)}) %all-to-all-start.4) | async-done | bytes 131104 | tf_op jit(solution)/shard_map/all_to_all | solution.py:151
  312.5 0.7 fusion.5
  (51 shorter events, 2.8 us)
Async XLA Ops:
  6.5 112.7 %copy-start = (bf16[4,1,1024,128]{3,2,1,0:T(8,128)(2,1)S(1)}, bf16[4,1,1024,128]{3,2,1,0:T(8,128)(2,1)}, u32[]{:S(2)}) copy-start(bf16[4,1,1024,128]{3,2,1,0:T(8,128)(2,1)} %param.19) | copy-start | bytes 3145732
  6.5 78.5 %all-gather.4.cloned.1.call-start = ((), (), s32[]{:S(2)}) async-start(), calls=%async_computation.5 | async-start | bytes 1114112 | tf_op jit(solution)/shard_map/all_gather | solution.py:22
  18.6 98.4 %all-gather.6.cloned.1.call-start = ((), (), s32[]{:S(2)}) async-start(), calls=%async_computation.6 | async-start | bytes 3145728 | tf_op jit(solution)/shard_map/all_gather | solution.py:22
  117.0 1.8 copy-start.3
  117.0 1.9 copy-start.5
  118.8 21.8 %copy-start.6 = (bf16[4,1,1024,128]{3,2,1,0:T(8,128)(2,1)S(1)}, bf16[4,1,1024,128]{3,2,1,0:T(8,128)(2,1)}, u32[]{:S(2)}) copy-start(bf16[4,1,1024,128]{3,2,1,0:T(8,128)(2,1)} %param.20) | copy-start | bytes 3145732
  140.6 45.6 %copy-start.4 = (bf16[512,16]{0,1:T(8,128)(2,1)S(1)}, bf16[512,16]{0,1:T(8,128)(2,1)}, u32[]{:S(2)}) copy-start(bf16[512,16]{0,1:T(8,128)(2,1)} %param.22) | copy-start | bytes 49156
  186.6 84.4 %copy-start.1 = (bf16[1,2048,192]{1,2,0:T(8,128)(2,1)S(1)}, bf16[1,2048,192]{1,2,0:T(8,128)(2,1)}, u32[]{:S(2)}) copy-start(bf16[1,2048,192]{1,2,0:T(8,128)(2,1)} %param.27) | copy-start | bytes 2359300
  201.8 31.9 %all-to-all-start = ((bf16[128,4,16]{2,1,0:T(4,128)(2,1)}), bf16[128,4,16]{2,1,0:T(4,128)(2,1)S(1)}, u32[]{:S(2)}, u32[]{:S(2)}) async-start(bf16[128,4,16]{2,1,0:T(4,128)(2,1)} %psum.7), calls=%async_computation | async-start | bytes 262144 | tf_op jit(solution)/shard_map/all_to_all | solution.py:122
  233.8 37.6 %copy-start.2 = (bf16[1,192,2048]{2,1,0:T(8,128)(2,1)S(1)}, bf16[1,192,2048]{2,1,0:T(8,128)(2,1)}, u32[]{:S(2)}) copy-start(bf16[1,192,2048]{2,1,0:T(8,128)(2,1)} %param.29) | copy-start | bytes 2359300
  273.5 22.8 %copy-start.7 = (bf16[4,2]{0,1:T(2,128)(2,1)S(1)}, bf16[4,2]{0,1:T(2,128)(2,1)}, u32[]{:S(2)}) copy-start(bf16[4,2]{0,1:T(2,128)(2,1)} %param.26) | copy-start | bytes 52
  284.8 27.6 %all-to-all-start.4 = ((bf16[128,2,256]{2,1,0:T(2,128)(2,1)}), bf16[128,2,256]{2,1,0:T(2,128)(2,1)S(1)}, u32[]{:S(2)}, u32[]{:S(2)}) async-start(bf16[128,2,256]{2,1,0:T(2,128)(2,1)} %reshape.171), calls=%async_computation.4 | async-start | bytes 262144 | tf_op jit(solution)/shard_map/all_to_all | solution.py:151
Sparse Core Ops, SparseCore 0:
  18.7 66.2 all-gather.3
  87.1 29.8 all-gather.5
where the time goes:
time: 321 us; the launch traced here: 320 us
  waiting for transfers between devices  126 us (39%)
  blocking collectives  118 us (37%)
  starting transfers between devices  27.4 us (9%)
  other arithmetic  24.6 us (8%)
  between operations  13.7 us (4%)
  local copies, waits for them, and re-layouts  5.95 us (2%)
  matrix products  4.82 us (2%)
    all_gather x2, waiting for transfers between devices, gather_in_order(): tiles = lax.all_gather(tiles, axes[k], axis=0, tiled=True)  93.9 us
    all_gather x4, blocking collectives, gather_in_order(): tiles = lax.all_gather(tiles, axes[k], axis=0, tiled=True)  56.9 us
    all_to_all x2, blocking collectives, moved_by_axis(): lax.all_to_all(tiles, axes[k], split_axis=k, concat_axis=k, tiled=True)  25.1 us
    another operation x2, other arithmetic  20.5 us
    all_to_all x1, waiting for transfers between devices, body(): lax.all_to_all(summed, EP, split_axis=0, concat_axis=0, tiled=True)  16.1 us
    all_to_all x1, starting transfers between devices, body(): lax.all_to_all(col_total.astype(jnp.bfloat16), EP, split_axis=0, concat_a...  15.9 us
    all_to_all x1, waiting for transfers between devices, body(): lax.all_to_all(col_total.astype(jnp.bfloat16), EP, split_axis=0, concat_a...  15.9 us
    psum x1, blocking collectives, body(): col_total = lax.psum(rounded.astype(jnp.bfloat16), 'tp').astype(jnp.float32)  15.2 us
  transfers between devices with their start and end apart: 4, of which 4 were waited for; matrix products, arithmetic and copies ran while one was open for 1% of the time, Pallas kernels for 0%

commit v1 on v0

v1 whole, which is shorter than its diff:
```python
import jax
import jax.numpy as jnp
from jax import lax
from jax.experimental import pallas as pl
from jax.experimental.pallas import tpu as pltpu
from jax.sharding import Mesh
from jax.sharding import PartitionSpec as P

EP = ("ep_0", "ep_1", "ep_2")
MESH = pl.DeviceIdType.MESH
F32 = jnp.float32
BF16 = jnp.bfloat16
NZ, NX, NC, NY = 16, 4, 2, 4
NXC = NX * NC
NSHORT = NXC * NY
EPS = 1e-06

NT = (((1,), (1,)), ((), ()))
TN = (((0,), (0,)), ((), ()))


def dot(a, b, dims=None, precision=None):
    if dims is None:
        dims = (((1,), (0,)), ((), ()))
    return lax.dot_general(a, b, dims, precision=precision, preferred_element_type=F32)


def iota(shape, dim):
    return lax.broadcasted_iota(jnp.int32, shape, dim)


def kernel(
    hid_ref,
    again_ref,
    wq_ref,
    bias_ref,
    k_hbm,
    v_hbm,
    len_ref,
    wo_ref,
    mgain_ref,
    rg_ref,
    ri_ref,
    rw_ref,
    gate_hbm,
    up_hbm,
    down_hbm,
    out_ref,
    k_v,
    v_v,
    wg_v,
    wu_v,
    wd_v,
    wq_g,
    wo_g,
    wo_t,
    sn,
    sh,
    sr,
    rn,
    rh,
    rr,
    sq,
    rq,
    so,
    ro,
    sp,
    rp,
    sd,
    rd,
    sx,
    rx,
    se,
    re,
    sf,
    rf,
    rres,
    load_sem,
    send_sem,
    recv_sem,
):
    z = lax.axis_index("ep_0")
    x = lax.axis_index("ep_1")
    c = lax.axis_index("ep_2")
    y = lax.axis_index("tp")
    xc = x * NC + c
    me = xc * NY + y

    loads = [
        pltpu.make_async_copy(k_hbm, k_v, load_sem.at[0]),
        pltpu.make_async_copy(v_hbm, v_v, load_sem.at[1]),
        pltpu.make_async_copy(down_hbm, wd_v, load_sem.at[2]),
    ]
    for half in range(2):
        loads.append(pltpu.make_async_copy(gate_hbm.at[:, half], wg_v.at[half], load_sem.at[3 + half]))
        loads.append(pltpu.make_async_copy(up_hbm.at[:, half], wu_v.at[half], load_sem.at[5 + half]))
    for one in loads:
        one.start()

    def z_of(i):
        off = (i + 1) // 2
        return (z + 8 + jnp.where(i % 2 == 1, NZ - off, off)) % NZ

    def short_of(j):
        p = (me + j) % NSHORT
        return p // NY, p % NY

    barrier = pltpu.get_barrier_semaphore()

    def greet_z(i, carry):
        pl.semaphore_signal(barrier, inc=1, device_id={"ep_0": z_of(i)}, device_id_type=MESH)
        return carry

    def greet_short(j, carry):
        pxc, py = short_of(j)
        pl.semaphore_signal(
            barrier, inc=1, device_id={"ep_1": pxc // NC, "ep_2": pxc % NC, "tp": py}, device_id_type=MESH
        )
        return carry

    lax.fori_loop(0, NZ - 1, greet_z, 0)
    lax.fori_loop(1, NSHORT, greet_short, 0)

    hid = hid_ref[...].astype(F32)
    scale = lax.rsqrt(jnp.mean(hid * hid, axis=-1, keepdims=True) + EPS)
    hid2 = jnp.concatenate([hid, hid], axis=0)
    scale2 = jnp.concatenate([scale, scale], axis=0)
    for k in range(NZ):
        part = hid2[:, 128 * k : 128 * k + 128]
        sn[k] = (part * scale2 * again_ref[k : k + 1, :]).astype(BF16)
        sh[k] = part.astype(BF16)

    eye = (iota((16, 16), 0) == iota((16, 16), 1)).astype(BF16)
    wo_t[...] = dot(eye, wo_ref[...], NT).astype(BF16)

    lane = iota((1, 128), 1)
    tok_a = lane % 4
    near = (lane // 4) == z
    wide = (lane // 8) == z
    route_w = rw_ref[...].astype(F32)
    rows = []
    for pattern in (near, wide):
        for k in range(2):
            row = jnp.zeros((1, 128), F32)
            for t in range(4):
                ident = (rg_ref[t] * 32 + ri_ref[2 * t + k]).astype(F32)
                row = jnp.where(tok_a == t, ident, row)
            rows.append(jnp.where(pattern, row, 0.0))
    for k in range(2):
        spread = jnp.where(
            (iota((4, 128), 1) % 4) == iota((4, 128), 0), jnp.broadcast_to(route_w[:, k : k + 1], (4, 128)), 0.0
        )
        rows.append(jnp.where(wide, jnp.sum(spread, axis=0, keepdims=True), 0.0))
    rowid = iota((8, 128), 0)
    packet = jnp.zeros((8, 128), F32)
    for k, row in enumerate(rows):
        packet = jnp.where(rowid == k, jnp.broadcast_to(row, (8, 128)), packet)
    sr[...] = packet.astype(BF16)

    pl.semaphore_wait(barrier, NZ - 1 + NSHORT - 1)

    def to_z(i, src, dst, phase):
        return pltpu.make_async_remote_copy(
            src_ref=src,
            dst_ref=dst,
            send_sem=send_sem.at[phase],
            recv_sem=recv_sem.at[phase],
            device_id={"ep_0": z_of(i)},
            device_id_type=MESH,
        )

    def to_short(pxc, py, src, dst, phase):
        return pltpu.make_async_remote_copy(
            src_ref=src,
            dst_ref=dst,
            send_sem=send_sem.at[phase],
            recv_sem=recv_sem.at[phase],
            device_id={"ep_1": pxc // NC, "ep_2": pxc % NC, "tp": py},
            device_id_type=MESH,
        )

    def all_of(ref, phase):
        return pltpu.make_async_remote_copy(
            src_ref=ref,
            dst_ref=ref,
            send_sem=send_sem.at[phase],
            recv_sem=recv_sem.at[phase],
            device_id={"ep_0": (z + 1) % NZ},
            device_id_type=MESH,
        )

    def z_exchange(src_of, dst, phase):
        def go(i, carry):
            to_z(i, src_of(z_of(i)), dst, phase).start()
            return carry

        lax.fori_loop(0, NZ - 1, go, 0)

    z_exchange(lambda p: sn.at[p], rn.at[z], 0)

    def gather_weights(src, dst, phase):
        def go(j, carry):
            p = (xc + j) % NXC
            to_short(p, y, src, dst.at[xc], phase).start()
            return carry

        lax.fori_loop(1, NXC, go, 0)

    gather_weights(wq_ref, wq_g, 1)
    z_exchange(lambda p: sr, rr.at[z], 3)
    z_exchange(lambda p: sh.at[p], rh.at[z], 2)
    gather_weights(wo_t, wo_g, 4)
    rn[z] = sn[z]
    rr[z] = sr[...]
    rh[z] = sh[z]
    wq_g[xc] = wq_ref[...]
    wo_g[xc] = wo_t[...]

    all_of(rn.at[0 : NZ - 1], 0).wait_recv()
    all_of(wq_g.at[0 : NXC - 1], 1).wait_recv()

    first = (iota((128, 128), 0) % 8) < 4
    xin = rn[...].astype(F32).reshape(128, 128).astype(BF16)
    wq_z = wq_g[...].reshape(128, 512)
    part_q = dot(xin, wq_z)
    for p in range(2):
        pair = jnp.where(first, part_q[:, 256 * p : 256 * p + 128], part_q[:, 256 * p + 128 : 256 * p + 256])
        sq[:, p] = pair.reshape(NZ, 8, 128).astype(BF16)
    z_exchange(lambda p: sq.at[p], rq.at[z], 5)
    rq[z] = sq[z]

    later = (iota((128, 128), 0) > iota((128, 128), 1)).astype(F32)
    rowh = iota((16, 1), 0)
    bias = jnp.zeros((16, 1), F32)
    length = jnp.zeros((16, 1), jnp.int32)
    for h in range(4):
        bias = jnp.where(rowh // 4 == h, bias_ref[4 * y + h], bias)
        length = jnp.where(rowh % 4 == h, len_ref[h], length)

    all_of(rq.at[0 : NZ - 1], 5).wait_recv()
    q = jnp.sum(rq[...].astype(F32), axis=0).reshape(16, 128).astype(BF16)
    loads[0].wait()
    tok = iota((16, 1024), 0) % 4
    scores = jnp.zeros((16, 1024), F32)
    for t in range(4):
        scores = jnp.where(tok == t, dot(q, k_v[t], NT), scores)
    scores = scores * (128.0 ** -0.5) + bias
    soft = jnp.log1p(jnp.exp(-jnp.abs(scores)))
    log_stop = jnp.minimum(scores, 0.0) - soft
    visible = iota((16, 1024), 1) < length
    log_keep = jnp.where(visible, log_stop - scores, 0.0)
    stacked = jnp.concatenate([log_keep[:, 128 * k : 128 * k + 128] for k in range(8)], axis=0)
    within = dot(stacked, later, precision=lax.Precision.HIGHEST)
    carry_sum = jnp.zeros((16, 1), F32)
    weights = [None] * 8
    for k in reversed(range(8)):
        inner = within[16 * k : 16 * k + 16]
        keep_k = log_keep[:, 128 * k : 128 * k + 128]
        expo = jnp.exp(log_stop[:, 128 * k : 128 * k + 128] + (inner + carry_sum))
        weights[k] = jnp.where(visible[:, 128 * k : 128 * k + 128], expo, 0.0)
        carry_sum = carry_sum + (inner[:, 0:1] + keep_k[:, 0:1])
    weight = jnp.concatenate(weights, axis=1).astype(BF16)
    loads[1].wait()
    tok_o = iota((16, 128), 0) % 4
    heads = jnp.zeros((16, 128), F32)
    for t in range(4):
        heads = jnp.where(tok_o == t, dot(weight, v_v[t]), heads)
    so[...] = heads.astype(BF16)

    z_exchange(lambda p: so, ro.at[z], 6)
    ro[z] = so[...]
    all_of(wo_g.at[0 : NXC - 1], 4).wait_recv()
    wo_z = wo_g[...].reshape(128, 512)
    head_row = (iota((256, 128), 0) % 16) // 4
    all_of(ro.at[0 : NZ - 1], 6).wait_recv()
    heads_in = ro[...].reshape(256, 128)
    proj = jnp.zeros((256, 128), F32)
    for h in range(4):
        proj = jnp.where(head_row == h, dot(heads_in, wo_z[:, 128 * h : 128 * h + 128], NT), proj)
    proj = jnp.sum(proj.reshape(NZ, 2, 8, 128), axis=1)
    proj = proj + pltpu.roll(proj, 4, 1)
    sp[...] = proj.reshape(4, 4, 8, 128).astype(BF16)

    def send_part(j, carry):
        py = (y + j) % NY
        to_short(xc, py, sp.at[py], rp.at[y], 7).start()
        return carry

    lax.fori_loop(1, NY, send_part, 0)
    rp[y] = sp[y]

    all_of(rr.at[0 : NZ - 1], 3).wait_recv()
    route = jnp.sum(rr[...].astype(F32), axis=0)
    mine = pltpu.roll(route, (128 - 16 * y) % 128, 1)
    slot_row = iota((64, 16), 0)
    slot_expert = (NXC * z + slot_row // 8).astype(F32)
    same_block = (slot_row % 4) == (iota((64, 16), 1) // 4)
    wanted = (mine[0:1, 0:16] == slot_expert) | (mine[1:2, 0:16] == slot_expert)
    select = jnp.where(same_block & wanted, 1.0, 0.0).astype(BF16)

    all_of(rh.at[0 : NZ - 1], 2).wait_recv()
    own_hidden = rh[pl.ds(4 * y, 4)].astype(F32)
    all_of(rp.at[0 : NY - 1], 7).wait_recv()
    resid = own_hidden + jnp.sum(rp[...].astype(F32), axis=0)
    first8 = iota((8, 128), 0) < 4
    sd[...] = jnp.concatenate(
        [jnp.where(first8, resid[0], resid[1]), jnp.where(first8, resid[2], resid[3])], axis=0
    ).astype(BF16)

    z_exchange(lambda p: sd, rd.at[z], 8)
    rd[z] = sd[...]

    crow = iota((256, 128), 0)
    clane = iota((256, 128), 1)
    cexp = (NXC * z + crow // 32).astype(F32)
    cblock = (crow // 8) % 4 * 4 + crow % 4
    cmatch = (cblock == clane // 8) & (((crow // 4) % 2) == ((clane // 4) % 2))
    cweight = jnp.where(route[2:3] == cexp, route[4:5], 0.0) + jnp.where(route[3:4] == cexp, route[5:6], 0.0)
    combine = jnp.where(cmatch, cweight, 0.0).astype(BF16)

    all_of(rd.at[0 : NZ - 1], 8).wait_recv()
    rows_in = rd[...].astype(F32)
    square = jnp.sum(jnp.sum(rows_in * rows_in, axis=0), axis=-1, keepdims=True) * (1.0 / 2048.0)
    scale_two = lax.rsqrt(square + EPS)
    normed = jnp.concatenate(
        [(rows_in[k] * scale_two * mgain_ref[k : k + 1, :]).astype(BF16) for k in range(NZ)], axis=1
    )
    slots = dot(select, normed)
    first64 = (iota((64, 128), 0) % 8) < 4
    for m in range(8):
        pair = jnp.where(first64, slots[:, 256 * m : 256 * m + 128], slots[:, 256 * m + 128 : 256 * m + 256])
        sx[:, m] = pair.reshape(NXC, 8, 128).astype(BF16)

    def send_slots(j, carry):
        pxc, py = short_of(j)
        to_short(pxc, py, sx.at[pxc], rx.at[me], 9).start()
        return carry

    lax.fori_loop(1, NSHORT, send_slots, 0)
    rx[me] = sx[xc]

    owner = z // 4

    @pl.when(y == owner)
    def _():
        def send_rows(j, carry):
            py = (y + j) % NY
            to_short(xc, py, rd.at[pl.ds(4 * py, 4)], rres, 12).start()
            return carry

        lax.fori_loop(1, NY, send_rows, 0)
        rres[...] = rd[pl.ds(4 * y, 4)]

    for one in loads[2:]:
        one.wait()
    all_of(rx.at[0 : NSHORT - 1], 9).wait_recv()
    lhs = jnp.concatenate([rx[:, m].astype(F32).reshape(256, 128).astype(BF16) for m in range(8)], axis=1)
    first_ff = (iota((256, 192), 0) % 8) < 4

    def swap(v):
        return pltpu.roll(v.reshape(32, 8, 192), 4, 1).reshape(256, 192)

    def both_halves(w):
        both = jnp.where(first_ff, dot(lhs, w[0].reshape(1024, 192)), dot(lhs, w[1].reshape(1024, 192)))
        return both + swap(both)

    gated = both_halves(wg_v)
    upped = both_halves(wu_v)
    act = (gated / (1.0 + jnp.exp(-gated)) * upped).astype(BF16)

    first256 = (iota((256, 128), 0) % 8) < 4
    for m in range(8):
        down_a = dot(act, wd_v[:, 256 * m : 256 * m + 128])
        down_b = dot(act, wd_v[:, 256 * m + 128 : 256 * m + 256])
        pair = jnp.where(first256, down_a, down_b).reshape(NXC, NY, 8, 128).astype(BF16)
        se[:, m // 2, m % 2] = pair

    def send_back(j, carry):
        pxc, py = short_of(j)
        to_short(pxc, py, se.at[pxc, py], re.at[me], 10).start()
        return carry

    lax.fori_loop(1, NSHORT, send_back, 0)
    re[me] = se[xc, y]

    all_of(re.at[0 : NSHORT - 1], 10).wait_recv()
    for m in range(2):
        total = jnp.sum(re[:, m].astype(F32).reshape(NXC, NY, NY * 8, 128), axis=1)
        total = total.reshape(256, 128).astype(BF16)
        mixed = dot(combine, total, TN)
        sf[:, m] = mixed.reshape(NZ, 8, 128).astype(BF16)

    z_exchange(lambda p: sf.at[p], rf.at[z], 11)
    rf[z] = sf[z]

    @pl.when(y != owner)
    def _():
        all_of(rres, 12).wait_recv()

    pick = (iota((4, 16), 1) == 4 * (z % 4) + iota((4, 16), 0)).astype(BF16)
    own_rows = [dot(pick, rres[k]) for k in range(4)]
    all_of(rf.at[0 : NZ - 1], 11).wait_recv()
    routed = jnp.sum(rf[...].astype(F32), axis=0).reshape(16, 128)
    for k in range(4):
        out_ref[:, 128 * k : 128 * k + 128] = (own_rows[k] + routed[4 * k : 4 * k + 4]).astype(BF16)

    for ref, phase in (
        (rn.at[0 : NZ - 1], 0),
        (wq_g.at[0 : NXC - 1], 1),
        (rh.at[0 : NZ - 1], 2),
        (rr.at[0 : NZ - 1], 3),
        (wo_g.at[0 : NXC - 1], 4),
        (rq.at[0 : NZ - 1], 5),
        (ro.at[0 : NZ - 1], 6),
        (rp.at[0 : NY - 1], 7),
        (rd.at[0 : NZ - 1], 8),
        (rx.at[0 : NSHORT - 1], 9),
        (re.at[0 : NSHORT - 1], 10),
        (rf.at[0 : NZ - 1], 11),
    ):
        all_of(ref, phase).wait_send()

    @pl.when(y == owner)
    def _():
        all_of(rd.at[0:12], 12).wait_send()


def body(
    hidden,
    attn_gain,
    query_weight,
    head_bias,
    key_cache,
    value_cache,
    lengths,
    out_weight,
    moe_gain,
    route_group,
    route_inner,
    route_weight,
    gate_w,
    up_w,
    down_w,
):
    vmem = pl.BlockSpec(memory_space=pltpu.VMEM)
    smem = pl.BlockSpec(memory_space=pltpu.SMEM)
    hbm = pl.BlockSpec(memory_space=pl.ANY)

    def buf(*shape):
        return pltpu.VMEM(shape, BF16)

    return pl.pallas_call(
        kernel,
        out_shape=jax.ShapeDtypeStruct((4, 512), BF16),
        in_specs=[vmem, vmem, vmem, smem, hbm, hbm, smem, vmem, vmem, smem, smem, vmem, hbm, hbm, hbm],
        out_specs=vmem,
        scratch_shapes=[
            buf(4, 1024, 128),
            buf(4, 1024, 128),
            buf(2, 8, 128, 192),
            buf(2, 8, 128, 192),
            buf(192, 2048),
            buf(NXC, 16, 512),
            buf(NXC, 16, 512),
            buf(16, 512),
            buf(NZ, 8, 128),
            buf(NZ, 8, 128),
            buf(8, 128),
            buf(NZ, 8, 128),
            buf(NZ, 8, 128),
            buf(NZ, 8, 128),
            buf(NZ, 2, 8, 128),
            buf(NZ, 2, 8, 128),
            buf(16, 128),
            buf(NZ, 16, 128),
            buf(NY, 4, 8, 128),
            buf(NY, 4, 8, 128),
            buf(16, 128),
            buf(NZ, 16, 128),
            buf(NXC, 8, 8, 128),
            buf(NSHORT, 8, 8, 128),
            buf(NXC, NY, 2, NY, 8, 128),
            buf(NSHORT, 2, NY, 8, 128),
            buf(NZ, 2, 8, 128),
            buf(NZ, 2, 8, 128),
            buf(4, 16, 128),
            pltpu.SemaphoreType.DMA((7,)),
            pltpu.SemaphoreType.DMA((13,)),
            pltpu.SemaphoreType.DMA((13,)),
        ],
        compiler_params=pltpu.CompilerParams(
            collective_id=0, has_side_effects=True, vmem_limit_bytes=40 * 1024 * 1024
        ),
        name="layer",
    )(
        hidden,
        attn_gain.reshape(16, 128),
        query_weight,
        head_bias,
        key_cache.reshape(4, 1024, 128),
        value_cache.reshape(4, 1024, 128),
        lengths,
        out_weight,
        moe_gain.reshape(16, 128),
        route_group,
        route_inner.reshape(8),
        route_weight,
        gate_w.reshape(8, 2, 128, 192),
        up_w.reshape(8, 2, 128, 192),
        down_w.reshape(192, 2048),
    )


def solution(mesh):
    torus = Mesh(mesh.devices.reshape(NZ, NX, NC, NY), ("ep_0", "ep_1", "ep_2", "tp"))
    placed = (
        P(EP, None),
        P(),
        P(EP, "tp"),
        P(),
        P(EP, "tp", None, None),
        P(EP, "tp", None, None),
        P(EP),
        P("tp", EP),
        P(),
        P(EP),
        P(EP, None),
        P(EP, None),
        P(EP, None, "tp"),
        P(EP, None, "tp"),
        P(EP, "tp", None),
    )
    return jax.shard_map(body, mesh=torus, in_specs=placed, out_specs=P(EP, "tp"), check_vma=False)
```

time: 321 us -> 84 us (0.26)
  waiting for transfers between devices: 126 us -> 0 us
  blocking collectives: 118 us -> 0 us
  Pallas kernels: 0 us -> 75.2 us
  starting transfers between devices: 27.4 us -> 0 us
  other arithmetic: 24.6 us -> 0 us
  between operations: 13.7 us -> 0.14 us
  matrix products: 4.82 us -> 0 us
    all_gather x2 -> x0, waiting for transfers between devices: 93.9 us -> none  [gather_in_order(): tiles = lax.all_gather(tiles, axes[k], axis=0, tiled=True)]
    pallas_call x0 -> x1, Pallas kernels: none -> 75.2 us  [body(): pl.pallas_call(kernel, out_shape=jax.ShapeDtypeStruct((4, 512), BF16), in...]
    all_gather x5 -> x0, blocking collectives: 68.1 us -> none  [the longest x4 56.9 us: gather_in_order(): tiles = lax.all_gather(tiles, axes[k], axis=0, tiled=True)]
    all_to_all x3 -> x0, blocking collectives: 34.4 us -> none  [the longest x2 25.1 us: moved_by_axis(): lax.all_to_all(tiles, axes[k], split_axis=k, concat_axis=k, tiled=True)]
    all_to_all x2 -> x0, waiting for transfers between devices: 32 us -> none  [the longest x1 16.1 us: body(): lax.all_to_all(summed, EP, split_axis=0, concat_axis=0, tiled=True)]
    all_to_all x2 -> x0, starting transfers between devices: 27.3 us -> none  [the longest x1 15.9 us: body(): lax.all_to_all(col_total.astype(jnp.bfloat16), EP, split_axis=0, concat_a...]
    another operation x2 -> x0, other arithmetic: 20.5 us -> none
    psum x1 -> x0, blocking collectives: 15.2 us -> none  [body(): col_total = lax.psum(rounded.astype(jnp.bfloat16), 'tp').astype(jnp.float32)]
  transfers between devices with their start and end apart: 4 -> 0, of which waited for: 4 -> 0; matrix products, arithmetic and copies ran while one was open for 1% -> 0% of each run, Pallas kernels for 0% -> 0%
where the time goes in v1:
time: 84 us; the launch traced here: 83.7 us
  Pallas kernels  75.2 us (90%)
  local copies, waits for them, and re-layouts  8.29 us (10%)
    pallas_call x1, Pallas kernels, body(): pl.pallas_call(kernel, out_shape=jax.ShapeDtypeStruct((4, 512), BF16), in...  75.2 us
    unnamed x28, local copies, waits for them, and re-layouts  8.21 us

profile of v1, /device:TPU:1, one launch (start us, length us, event | category | flops | bytes accessed | tf_op | source)
XLA Modules:
  0.0 83.7 jit_solution(7876358231525558664)
XLA Ops:
  0.0 0.0 copy-start.10
  0.0 0.8 copy.25.rw_ref
  0.8 0.8 copy.21
  1.5 0.1 reshape.28.ri_ref
  1.6 0.0 copy-done.10
  1.6 0.1 copy.24.wo_ref
  1.8 1.4 %copy.22 = bf16[1,2048,192]{2,1,0:T(8,128)(2,1)S(1)} copy(bf16[1,2048,192]{1,2,0:T(8,128)(2,1)} %param.27) | data formatting | bytes 1572864 | tf_op args[12]
  3.2 0.0 copy-start
  3.2 0.0 copy-start.3
  3.2 0.0 copy-start.4
  3.2 0.0 copy-start.5
  3.2 0.0 copy-start.6
  3.3 1.5 %copy.23 = bf16[1,2048,192]{2,1,0:T(8,128)(2,1)S(1)} copy(bf16[1,2048,192]{1,2,0:T(8,128)(2,1)} %param.28) | data formatting | bytes 1572864 | tf_op args[13]
  4.8 0.0 copy-start.7
  4.8 0.0 copy-start.8
  4.8 0.0 copy-start.9
  4.8 0.0 copy-done
  4.8 0.0 copy-done.3
  4.8 0.0 copy-done.4
  4.8 0.0 copy-done.5
  4.9 0.0 copy-done.6
  4.9 0.6 copy-done.7
  5.4 0.0 copy-done.8
  5.5 0.0 copy-done.9
  5.5 0.0 copy-start.1
  5.5 1.2 %copy-done.1 = bf16[4,1,1024,128]{3,2,1,0:T(8,128)(2,1)S(1)} copy-done((bf16[4,1,1024,128]{3,2,1,0:T(8,128)(2,1)S(1)}, bf16[4,1,1024,128]{3,2,1,0:T(8,128)(2,1)}, u32[]{:S(2)}) %copy-start.1) | copy-done | bytes 1048600
  6.7 0.0 copy-start.2
  6.7 1.1 %copy-done.2 = bf16[1,192,2048]{2,1,0:T(8,128)(2,1)S(1)} copy-done((bf16[1,192,2048]{2,1,0:T(8,128)(2,1)S(1)}, bf16[1,192,2048]{2,1,0:T(8,128)(2,1)}, u32[]{:S(2)}) %copy-start.2) | copy-done | bytes 786456
  7.8 75.2 %layer.1 = bf16[4,512]{1,0:T(4,128)(2,1)S(1)} custom-call(bf16[4,2048]{1,0:T(4,128)(2,1)S(1)} %copy-done.3, f32[16,128]{1,0:T(8,128)S(1)} %bitcast.12, bf16[16,512]{1,0:T(8,128)(2,1)S(1)} %copy-done.4, f32[16]{0:T(128)S(1)} %copy-done.7, bf16[4,1024,128]{2,1,0:T(8,128)(2,1)S(1)} %bitcast.9, bf16[4,1024,128]{2,1,0:T(8,128)(2,1)S(1)} %bitcast.10, ...), custom_call_target="tpu_custom_call" | custom-call | tf_op jit(solution)/shard_map/layer/pallas_call | solution.py:452
  83.1 0.6 copy.27
Async XLA Ops:
  0.0 1.6 %copy-start.10 = (bf16[512,16]{0,1:T(8,128)(2,1)S(1)}, bf16[512,16]{0,1:T(8,128)(2,1)}, u32[]{:S(2)}) copy-start(bf16[512,16]{0,1:T(8,128)(2,1)} %param.22) | copy-start | bytes 49156
  3.2 1.6 %copy-start = (bf16[4,1,1024,128]{3,2,1,0:T(8,128)(2,1)S(1)}, bf16[4,1,1024,128]{3,2,1,0:T(8,128)(2,1)}, u32[]{:S(2)}) copy-start(bf16[4,1,1024,128]{3,2,1,0:T(8,128)(2,1)} %param.19) | copy-start | bytes 3145732
  3.2 1.6 %copy-start.3 = (bf16[4,2048]{1,0:T(4,128)(2,1)S(1)}, bf16[4,2048]{1,0:T(4,128)(2,1)}, u32[]{:S(2)}) copy-start(bf16[4,2048]{1,0:T(4,128)(2,1)} %hid_ref.1) | copy-start | bytes 49156
  3.2 1.6 %copy-start.4 = (bf16[16,512]{1,0:T(8,128)(2,1)S(1)}, bf16[16,512]{1,0:T(8,128)(2,1)}, u32[]{:S(2)}) copy-start(bf16[16,512]{1,0:T(8,128)(2,1)} %wq_ref.1) | copy-start | bytes 49156
  3.2 1.6 %copy-start.5 = (f32[2048]{0:T(1024)S(1)}, f32[2048]{0:T(1024)}, u32[]{:S(2)}) copy-start(f32[2048]{0:T(1024)} %param.16) | copy-start | bytes 24580
  3.2 1.6 %copy-start.6 = (f32[2048]{0:T(1024)S(1)}, f32[2048]{0:T(1024)}, u32[]{:S(2)}) copy-start(f32[2048]{0:T(1024)} %param.23) | copy-start | bytes 24580
  4.8 0.7 copy-start.7
  4.8 0.7 copy-start.8
  4.8 0.7 copy-start.9
  5.5 1.2 %copy-start.1 = (bf16[4,1,1024,128]{3,2,1,0:T(8,128)(2,1)S(1)}, bf16[4,1,1024,128]{3,2,1,0:T(8,128)(2,1)}, u32[]{:S(2)}) copy-start(bf16[4,1,1024,128]{3,2,1,0:T(8,128)(2,1)} %param.20) | copy-start | bytes 3145732
  6.7 1.1 %copy-start.2 = (bf16[1,192,2048]{2,1,0:T(8,128)(2,1)S(1)}, bf16[1,192,2048]{2,1,0:T(8,128)(2,1)}, u32[]{:S(2)}) copy-start(bf16[1,192,2048]{2,1,0:T(8,128)(2,1)} %param.29) | copy-start | bytes 2359300

commit v2 on v1

--- a/solution.py
+++ b/solution.py
@@ -30,22 +30,32 @@
 
 
 def kernel(
+    hid_hbm,
+    again_hbm,
+    wq_hbm,
+    bias_hbm,
+    k_hbm,
+    v_hbm,
+    len_hbm,
+    wo_hbm,
+    mgain_hbm,
+    rg_hbm,
+    ri_hbm,
+    rw_hbm,
+    gate_hbm,
+    up_hbm,
+    down_hbm,
+    out_ref,
     hid_ref,
     again_ref,
     wq_ref,
     bias_ref,
-    k_hbm,
-    v_hbm,
     len_ref,
-    wo_ref,
+    wo_t,
     mgain_ref,
     rg_ref,
     ri_ref,
     rw_ref,
-    gate_hbm,
-    up_hbm,
-    down_hbm,
-    out_ref,
     k_v,
     v_v,
     wg_v,
@@ -53,7 +63,6 @@
     wd_v,
     wq_g,
     wo_g,
-    wo_t,
     sn,
     sh,
     sr,
@@ -86,17 +95,6 @@
     xc = x * NC + c
     me = xc * NY + y
 
-    loads = [
-        pltpu.make_async_copy(k_hbm, k_v, load_sem.at[0]),
-        pltpu.make_async_copy(v_hbm, v_v, load_sem.at[1]),
-        pltpu.make_async_copy(down_hbm, wd_v, load_sem.at[2]),
-    ]
-    for half in range(2):
-        loads.append(pltpu.make_async_copy(gate_hbm.at[:, half], wg_v.at[half], load_sem.at[3 + half]))
-        loads.append(pltpu.make_async_copy(up_hbm.at[:, half], wu_v.at[half], load_sem.at[5 + half]))
-    for one in loads:
-        one.start()
-
     def z_of(i):
         off = (i + 1) // 2
         return (z + 8 + jnp.where(i % 2 == 1, NZ - off, off)) % NZ
@@ -120,6 +118,29 @@
 
     lax.fori_loop(0, NZ - 1, greet_z, 0)
     lax.fori_loop(1, NSHORT, greet_short, 0)
+
+    copies = (
+        (hid_hbm, hid_ref),
+        (again_hbm, again_ref),
+        (rw_hbm, rw_ref),
+        (rg_hbm, rg_ref),
+        (ri_hbm, ri_ref),
+        (wq_hbm, wq_ref),
+        (wo_hbm, wo_t),
+        (bias_hbm, bias_ref),
+        (len_hbm, len_ref),
+        (mgain_hbm, mgain_ref),
+        (k_hbm, k_v),
+        (v_hbm, v_v),
+        (gate_hbm, wg_v),
+        (up_hbm, wu_v),
+        (down_hbm, wd_v),
+    )
+    loads = [pltpu.make_async_copy(src, dst, load_sem.at[i]) for i, (src, dst) in enumerate(copies)]
+    for one in loads:
+        one.start()
+    for one in loads[0:5]:
+        one.wait()
 
     hid = hid_ref[...].astype(F32)
     scale = lax.rsqrt(jnp.mean(hid * hid, axis=-1, keepdims=True) + EPS)
@@ -129,9 +150,6 @@
         part = hid2[:, 128 * k : 128 * k + 128]
         sn[k] = (part * scale2 * again_ref[k : k + 1, :]).astype(BF16)
         sh[k] = part.astype(BF16)
-
-    eye = (iota((16, 16), 0) == iota((16, 16), 1)).astype(BF16)
-    wo_t[...] = dot(eye, wo_ref[...], NT).astype(BF16)
 
     lane = iota((1, 128), 1)
     tok_a = lane % 4
@@ -143,20 +161,22 @@
         for k in range(2):
             row = jnp.zeros((1, 128), F32)
             for t in range(4):
-                ident = (rg_ref[t] * 32 + ri_ref[2 * t + k]).astype(F32)
+                ident = (rg_ref[t] * 32 + ri_ref[k, t]).astype(F32)
                 row = jnp.where(tok_a == t, ident, row)
             rows.append(jnp.where(pattern, row, 0.0))
     for k in range(2):
-        spread = jnp.where(
-            (iota((4, 128), 1) % 4) == iota((4, 128), 0), jnp.broadcast_to(route_w[:, k : k + 1], (4, 128)), 0.0
-        )
-        rows.append(jnp.where(wide, jnp.sum(spread, axis=0, keepdims=True), 0.0))
+        row = jnp.zeros((1, 128), F32)
+        for t in range(4):
+            row = jnp.where(tok_a == t, route_w[k : k + 1, t : t + 1], row)
+        rows.append(jnp.where(wide, row, 0.0))
     rowid = iota((8, 128), 0)
     packet = jnp.zeros((8, 128), F32)
     for k, row in enumerate(rows):
         packet = jnp.where(rowid == k, jnp.broadcast_to(row, (8, 128)), packet)
     sr[...] = packet.astype(BF16)
 
+    for one in loads[5:10]:
+        one.wait()
     pl.semaphore_wait(barrier, NZ - 1 + NSHORT - 1)
 
     def to_z(i, src, dst, phase):
@@ -239,7 +259,7 @@
 
     all_of(rq.at[0 : NZ - 1], 5).wait_recv()
     q = jnp.sum(rq[...].astype(F32), axis=0).reshape(16, 128).astype(BF16)
-    loads[0].wait()
+    loads[10].wait()
     tok = iota((16, 1024), 0) % 4
     scores = jnp.zeros((16, 1024), F32)
     for t in range(4):
@@ -260,7 +280,7 @@
         weights[k] = jnp.where(visible[:, 128 * k : 128 * k + 128], expo, 0.0)
         carry_sum = carry_sum + (inner[:, 0:1] + keep_k[:, 0:1])
     weight = jnp.concatenate(weights, axis=1).astype(BF16)
-    loads[1].wait()
+    loads[11].wait()
     tok_o = iota((16, 128), 0) % 4
     heads = jnp.zeros((16, 128), F32)
     for t in range(4):
@@ -328,7 +348,7 @@
     slots = dot(select, normed)
     first64 = (iota((64, 128), 0) % 8) < 4
     for m in range(8):
-        pair = jnp.where(first64, slots[:, 256 * m : 256 * m + 128], slots[:, 256 * m + 128 : 256 * m + 256])
+        pair = jnp.where(first64, slots[:, 128 * m : 128 * m + 128], slots[:, 1024 + 128 * m : 1152 + 128 * m])
         sx[:, m] = pair.reshape(NXC, 8, 128).astype(BF16)
 
     def send_slots(j, carry):
@@ -351,7 +371,7 @@
         lax.fori_loop(1, NY, send_rows, 0)
         rres[...] = rd[pl.ds(4 * y, 4)]
 
-    for one in loads[2:]:
+    for one in loads[12:]:
         one.wait()
     all_of(rx.at[0 : NSHORT - 1], 9).wait_recv()
     lhs = jnp.concatenate([rx[:, m].astype(F32).reshape(256, 128).astype(BF16) for m in range(8)], axis=1)
@@ -361,7 +381,7 @@
         return pltpu.roll(v.reshape(32, 8, 192), 4, 1).reshape(256, 192)
 
     def both_halves(w):
-        both = jnp.where(first_ff, dot(lhs, w[0].reshape(1024, 192)), dot(lhs, w[1].reshape(1024, 192)))
+        both = jnp.where(first_ff, dot(lhs, w[:, 0:1024], NT), dot(lhs, w[:, 1024:2048], NT))
         return both + swap(both)
 
     gated = both_halves(wg_v)
@@ -443,8 +463,7 @@
     down_w,
 ):
     vmem = pl.BlockSpec(memory_space=pltpu.VMEM)
-    smem = pl.BlockSpec(memory_space=pltpu.SMEM)
-    hbm = pl.BlockSpec(memory_space=pl.ANY)
+    hbm = pl.BlockSpec(memory_space=pltpu.HBM)
 
     def buf(*shape):
         return pltpu.VMEM(shape, BF16)
@@ -452,17 +471,26 @@
     return pl.pallas_call(
         kernel,
         out_shape=jax.ShapeDtypeStruct((4, 512), BF16),
-        in_specs=[vmem, vmem, vmem, smem, hbm, hbm, smem, vmem, vmem, smem, smem, vmem, hbm, hbm, hbm],
+        in_specs=[hbm] * 15,
         out_specs=vmem,
         scratch_shapes=[
+            buf(4, 2048),
+            pltpu.VMEM((16, 128), F32),
+            buf(16, 512),
+            pltpu.SMEM((16,), F32),
+            pltpu.SMEM((4,), jnp.int32),
+            buf(16, 512),
+            pltpu.VMEM((16, 128), F32),
+            pltpu.SMEM((4,), jnp.int32),
+            pltpu.SMEM((2, 4), jnp.int32),
+            buf(2, 4),
             buf(4, 1024, 128),
             buf(4, 1024, 128),
-            buf(2, 8, 128, 192),
-            buf(2, 8, 128, 192),
+            buf(192, 2048),
+            buf(192, 2048),
             buf(192, 2048),
             buf(NXC, 16, 512),
             buf(NXC, 16, 512),
-            buf(16, 512),
             buf(NZ, 8, 128),
             buf(NZ, 8, 128),
             buf(8, 128),
@@ -484,12 +512,12 @@
             buf(NZ, 2, 8, 128),
             buf(NZ, 2, 8, 128),
             buf(4, 16, 128),
-            pltpu.SemaphoreType.DMA((7,)),
+            pltpu.SemaphoreType.DMA((15,)),
             pltpu.SemaphoreType.DMA((13,)),
             pltpu.SemaphoreType.DMA((13,)),
         ],
         compiler_params=pltpu.CompilerParams(
-            collective_id=0, has_side_effects=True, vmem_limit_bytes=40 * 1024 * 1024
+            collective_id=0, has_side_effects=True, vmem_limit_bytes=67043328
         ),
         name="layer",
     )(
@@ -500,13 +528,13 @@
         key_cache.reshape(4, 1024, 128),
         value_cache.reshape(4, 1024, 128),
         lengths,
-        out_weight,
+        out_weight.T,
         moe_gain.reshape(16, 128),
         route_group,
-        route_inner.reshape(8),
-        route_weight,
-        gate_w.reshape(8, 2, 128, 192),
-        up_w.reshape(8, 2, 128, 192),
+        route_inner.T,
+        route_weight.T,
+        jnp.swapaxes(gate_w, 1, 2).reshape(192, 2048),
+        jnp.swapaxes(up_w, 1, 2).reshape(192, 2048),
         down_w.reshape(192, 2048),
     )
 

time: 84 us -> 76.6 us (0.912)
  local copies, waits for them, and re-layouts: 8.29 us -> 1.28 us
    unnamed x28 -> x1, local copies, waits for them, and re-layouts: 8.21 us -> 1.28 us
where the time goes in v2:
time: 76.6 us; the launch traced here: 76.3 us
  Pallas kernels  75 us (98%)
  local copies, waits for them, and re-layouts  1.28 us (2%)
    pallas_call x1, Pallas kernels, body(): pl.pallas_call(kernel, out_shape=jax.ShapeDtypeStruct((4, 512), BF16), in...  75 us

profile of v2, /device:TPU:1, one launch (start us, length us, event | category | flops | bytes accessed | tf_op | source)
XLA Modules:
  0.0 76.3 jit_solution(10660896957169712213)
XLA Ops:
  0.0 75.0 %layer.1 = bf16[4,512]{1,0:T(4,128)(2,1)} custom-call(bf16[4,2048]{1,0:T(4,128)(2,1)} %hid_hbm.1, f32[16,128]{1,0:T(8,128)} %bitcast.20, bf16[16,512]{1,0:T(8,128)(2,1)} %wq_hbm.1, f32[16]{0:T(128)} %bias_hbm.1, bf16[4,1024,128]{2,1,0:T(8,128)(2,1)} %bitcast.14, bf16[4,1024,128]{2,1,0:T(8,128)(2,1)} %bitcast.15, s32[4]{0:T(128)} %len_hbm.1, ...), custom_call_target="tpu_custom_call" | custom-call | tf_op jit(solution)/shard_map/layer/pallas_call | solution.py:471
  75.0 1.3 %copy.17 = bf16[4,512]{1,0:T(4,128)(2,1)} copy(bf16[4,512]{1,0:T(4,128)(2,1)} %layer.1) | data formatting | bytes 8192

commit v3 on v2

v3 whole, which is shorter than its diff:
```python
import jax
import jax.numpy as jnp
from jax import lax
from jax.experimental import pallas as pl
from jax.experimental.pallas import tpu as pltpu
from jax.sharding import Mesh
from jax.sharding import PartitionSpec as P

EP = ("ep_0", "ep_1", "ep_2")
MESH = pl.DeviceIdType.MESH
F32 = jnp.float32
BF16 = jnp.bfloat16
NZ, NX, NC, NY = 16, 4, 2, 4
NXC = NX * NC
NSHORT = NXC * NY
EPS = 1e-06

Z_ORDER = (8, 7, 9, 6, 10, 5, 11, 4, 12, 3, 13, 2, 14, 1, 15)
HOPS = (0, 1, 2, 1)
XC_ORDER = sorted(((dx, dc) for dx in range(NX) for dc in range(NC) if dx or dc), key=lambda d: (-HOPS[d[0]], d))
SHORT_ORDER = sorted(
    ((dx, dc, dy) for dx in range(NX) for dc in range(NC) for dy in range(NY) if dx or dc or dy),
    key=lambda d: (-HOPS[d[0]] - HOPS[d[2]], d),
)

NT = (((1,), (1,)), ((), ()))
TN = (((0,), (0,)), ((), ()))


def dot(a, b, dims=None, precision=None):
    if dims is None:
        dims = (((1,), (0,)), ((), ()))
    return lax.dot_general(a, b, dims, precision=precision, preferred_element_type=F32)


def iota(shape, dim):
    return lax.broadcasted_iota(jnp.int32, shape, dim)


def kernel(
    hid_hbm,
    again_hbm,
    wq_hbm,
    bias_hbm,
    k_hbm,
    v_hbm,
    len_hbm,
    wo_hbm,
    mgain_hbm,
    rg_hbm,
    ri_hbm,
    rw_hbm,
    gate_hbm,
    up_hbm,
    down_hbm,
    out_ref,
    hid_ref,
    again_ref,
    wq_ref,
    bias_ref,
    len_ref,
    wo_t,
    mgain_ref,
    rg_ref,
    ri_ref,
    rw_ref,
    k_v,
    v_v,
    wg_v,
    wu_v,
    wd_v,
    wq_g,
    wo_r,
    wo_g,
    sn,
    sh,
    sr,
    rn,
    rh,
    rr,
    sq,
    rq,
    so,
    ro,
    sd,
    rd,
    sx,
    rx,
    se,
    re,
    sf,
    rf,
    load_sem,
    send_sem,
    recv_sem,
):
    z = lax.axis_index("ep_0")
    x = lax.axis_index("ep_1")
    c = lax.axis_index("ep_2")
    y = lax.axis_index("tp")
    xc = x * NC + c
    me = xc * NY + y

    def z_at(off):
        return lax.rem(z + off, NZ)

    def xc_at(dx, dc):
        return lax.rem(x + dx, NX), lax.rem(c + dc, NC)

    def y_at(dy):
        return lax.rem(y + dy, NY)

    barrier = pltpu.get_barrier_semaphore()

    def greet(device):
        pl.semaphore_signal(barrier, inc=1, device_id=device, device_id_type=MESH)

    for off in Z_ORDER:
        greet((z_at(off), x, c, y))
    for dx, dc in XC_ORDER:
        greet((z, *xc_at(dx, dc), y))
    for dy in range(1, NY):
        greet((z, x, c, y_at(dy)))
    greeted = NZ - 1 + NXC - 1 + NY - 1

    copies = (
        (hid_hbm, hid_ref),
        (again_hbm, again_ref),
        (rw_hbm, rw_ref),
        (rg_hbm, rg_ref),
        (ri_hbm, ri_ref),
        (wq_hbm, wq_ref),
        (wo_hbm, wo_t),
        (bias_hbm, bias_ref),
        (len_hbm, len_ref),
        (mgain_hbm, mgain_ref),
        (k_hbm, k_v),
        (v_hbm, v_v),
        (gate_hbm, wg_v),
        (up_hbm, wu_v),
        (down_hbm, wd_v),
    )
    loads = [pltpu.make_async_copy(src, dst, load_sem.at[i]) for i, (src, dst) in enumerate(copies)]
    for one in loads:
        one.start()
    for one in loads[0:5]:
        one.wait()

    hid = hid_ref[...].astype(F32)
    scale = lax.rsqrt(jnp.mean(hid * hid, axis=-1, keepdims=True) + EPS)
    hid2 = jnp.concatenate([hid, hid], axis=0)
    scale2 = jnp.concatenate([scale, scale], axis=0)
    for k in range(NZ):
        part = hid2[:, 128 * k : 128 * k + 128]
        sn[k] = (part * scale2 * again_ref[k : k + 1, :]).astype(BF16)
        sh[k] = part.astype(BF16)

    lane = iota((1, 128), 1)
    tok_a = lane % 4
    near = (lane % 64) // 4 == z
    wide = lane // 8 == z
    route_w = rw_ref[...].astype(F32)
    rows = []
    for pattern in (near, wide):
        for k in range(2):
            row = jnp.zeros((1, 128), F32)
            for t in range(4):
                ident = (rg_ref[t] * 32 + ri_ref[k, t]).astype(F32)
                row = jnp.where(tok_a == t, ident, row)
            rows.append(jnp.where(pattern, row, 0.0))
    for k in range(2):
        row = jnp.zeros((1, 128), F32)
        for t in range(4):
            row = jnp.where(tok_a == t, route_w[k : k + 1, t : t + 1], row)
        rows.append(jnp.where(wide, row, 0.0))
    rowid = iota((8, 128), 0)
    packet = jnp.zeros((8, 128), F32)
    for k, row in enumerate(rows):
        packet = jnp.where(rowid == k, jnp.broadcast_to(row, (8, 128)), packet)
    sr[...] = packet.astype(BF16)

    for one in loads[5:10]:
        one.wait()
    pl.semaphore_wait(barrier, greeted)

    def send(device, src, dst, phase):
        pltpu.make_async_remote_copy(
            src_ref=src,
            dst_ref=dst,
            send_sem=send_sem.at[phase],
            recv_sem=recv_sem.at[phase],
            device_id=device,
            device_id_type=MESH,
        ).start()

    def all_of(ref, phase):
        return pltpu.make_async_remote_copy(
            src_ref=ref,
            dst_ref=ref,
            send_sem=send_sem.at[phase],
            recv_sem=recv_sem.at[phase],
            device_id=(z_at(1), x, c, y),
            device_id_type=MESH,
        )

    def gather_line(src_of, dst, phase):
        for off in Z_ORDER:
            send((z_at(off), x, c, y), src_of(off), dst.at[NZ - off], phase)

    gather_line(lambda off: sn.at[z_at(off)], rn, 0)
    for dx, dc in XC_ORDER:
        send((z, *xc_at(dx, dc), y), wq_ref, wq_g.at[xc], 1)
    quad = lax.div(z, 4)
    for off in (8, 4, 12):
        send((z_at(off), x, c, y), wo_t, wo_r.at[quad], 4)
    gather_line(lambda off: sr, rr, 3)

    def near_chunk(off):
        return lax.rem(z + off, 4) + 4 * y

    for i in range(4):
        if i != 2:
            off = (2 - i) % NZ
            send((z_at(off), x, c, y), sh.at[near_chunk(off)], rh.at[i], 2)
    rn[0] = sn[z]
    rr[0] = sr[...]
    rh[2] = sh[near_chunk(0)]
    wq_g[xc] = wq_ref[...]
    wo_r[quad] = wo_t[...]

    all_of(rn.at[1:NZ], 0).wait_recv()
    all_of(wq_g.at[1:NXC], 1).wait_recv()

    first = (iota((128, 128), 0) % 8) < 4
    xin = rn[...].astype(F32).reshape(128, 128).astype(BF16)
    part_q = dot(xin, wq_g[...].reshape(128, 512))
    for p in range(2):
        pair = jnp.where(first, part_q[:, 256 * p : 256 * p + 128], part_q[:, 256 * p + 128 : 256 * p + 256])
        sq[:, p] = pair.reshape(NZ, 8, 128).astype(BF16)
    gather_line(lambda off: sq.at[off], rq, 5)
    rq[0] = sq[0]

    all_of(wo_r.at[1:4], 4).wait_recv()
    for dx, dc, dy in SHORT_ORDER:
        p = y_at(dy)
        send((z, *xc_at(dx, dc), p), wo_r.at[p], wo_g.at[y * NXC + xc], 7)
    wo_g[y * NXC + xc] = wo_r[y]

    later = (iota((128, 128), 0) > iota((128, 128), 1)).astype(F32)
    rowh = iota((16, 1), 0)
    bias = jnp.zeros((16, 1), F32)
    length = jnp.zeros((16, 1), jnp.int32)
    for h in range(4):
        bias = jnp.where(rowh // 4 == h, bias_ref[4 * y + h], bias)
        length = jnp.where(rowh % 4 == h, len_ref[h], length)

    all_of(rq.at[1:NZ], 5).wait_recv()
    q = jnp.sum(rq[...].astype(F32), axis=0).reshape(16, 128).astype(BF16)
    loads[10].wait()
    tok = iota((16, 1024), 0) % 4
    scores = jnp.zeros((16, 1024), F32)
    for t in range(4):
        scores = jnp.where(tok == t, dot(q, k_v[t], NT), scores)
    scores = scores * (128.0 ** -0.5) + bias
    soft = jnp.log1p(jnp.exp(-jnp.abs(scores)))
    log_stop = jnp.minimum(scores, 0.0) - soft
    visible = iota((16, 1024), 1) < length
    log_keep = jnp.where(visible, log_stop - scores, 0.0)
    stacked = jnp.concatenate([log_keep[:, 128 * k : 128 * k + 128] for k in range(8)], axis=0)
    within = dot(stacked, later, precision=lax.Precision.HIGHEST)
    carry_sum = jnp.zeros((16, 1), F32)
    weights = [None] * 8
    for k in reversed(range(8)):
        inner = within[16 * k : 16 * k + 16]
        keep_k = log_keep[:, 128 * k : 128 * k + 128]
        expo = jnp.exp(log_stop[:, 128 * k : 128 * k + 128] + (inner + carry_sum))
        weights[k] = jnp.where(visible[:, 128 * k : 128 * k + 128], expo, 0.0)
        carry_sum = carry_sum + (inner[:, 0:1] + keep_k[:, 0:1])
    weight = jnp.concatenate(weights, axis=1).astype(BF16)
    loads[11].wait()
    tok_o = iota((16, 128), 0) % 4
    heads = jnp.zeros((16, 128), F32)
    for t in range(4):
        heads = jnp.where(tok_o == t, dot(weight, v_v[t]), heads)
    so[...] = heads.astype(BF16)

    for dy in (2, 1, 3, 0):
        for i in (0, 1, 3, 2):
            if dy or i != 2:
                send((z_at((2 - i) % NZ), x, c, y_at(dy)), so, ro.at[4 * y + i], 6)
    ro[4 * y + 2] = so[...]

    all_of(rr.at[1:NZ], 3).wait_recv()
    route = jnp.sum(rr[...].astype(F32), axis=0)
    ids = pltpu.roll(route, lax.rem(4 * (NZ + 4 - z), 128), 1)
    wides = pltpu.roll(route, lax.rem(8 * (NZ + 4 - z), 128), 1)

    def select_of(g, start, count):
        shape = (64, 16 * count)
        row = iota(shape, 0)
        expert = (NXC * z + row // 8).astype(F32)
        same = iota(shape, 1) // 4 + (start - 6) == 8 * g + row % 8
        own = pltpu.roll(ids, (4 * (6 - start)) % 128, 1)
        wanted = (own[0:1, 0 : 16 * count] == expert) | (own[1:2, 0 : 16 * count] == expert)
        return jnp.where(same & wanted, 1.0, 0.0).astype(BF16)

    starts = ((4, 3), (5, 3), (6, 2), (3, 3))
    selects = [[select_of(g, start + 8 * g, count) for start, count in starts] for g in range(2)]

    def combine_of(g):
        row = iota((128, 64), 0)
        col = iota((128, 64), 1)
        expert = (NXC * z + (row // 8) % NXC).astype(F32)
        same = (row % 8 == col // 8) & (row // 64 == (col // 4) % 2)
        own = wides[:, 64 * g : 64 * g + 64]
        weight = jnp.where(own[2:3] == expert, own[4:5], 0.0) + jnp.where(own[3:4] == expert, own[5:6], 0.0)
        return jnp.where(same, weight, 0.0).astype(BF16)

    combines = [combine_of(g) for g in range(2)]

    all_of(rh.at[1:4], 2).wait_recv()
    all_of(wo_g.at[1:NSHORT], 7).wait_recv()
    all_of(ro.at[1:NZ], 6).wait_recv()
    head_row = (iota((64, 128), 0) % 16) // 4
    resid = rh[...].astype(F32)
    for p in range(NY):
        heads_in = ro[4 * p : 4 * p + 4].reshape(64, 128)
        wo_p = wo_g[NXC * p : NXC * p + NXC].reshape(128, 512)
        proj = jnp.zeros((64, 128), F32)
        for h in range(4):
            proj = jnp.where(head_row == h, dot(heads_in, wo_p[:, 128 * h : 128 * h + 128], NT), proj)
        proj = jnp.sum(proj.reshape(4, 2, 8, 128), axis=1)
        proj = proj + pltpu.roll(proj, 4, 1)
        resid = resid + proj.astype(BF16).astype(F32)
    first8 = iota((8, 128), 0) < 4
    sd[...] = jnp.concatenate(
        [jnp.where(first8, resid[0], resid[1]), jnp.where(first8, resid[2], resid[3])], axis=0
    ).astype(BF16)

    for off in Z_ORDER:
        send((z_at(off), x, c, y), sd, rd.at[(8 - off) % NZ], 12 if 6 <= off <= 10 else 8)
    rd[8] = sd[...]

    def to_experts(g, phase):
        for q, (start, count) in enumerate(starts):
            rows = jnp.concatenate([rd[(start + 8 * g + 4 * k) % NZ] for k in range(count)], axis=0)
            slots = dot(selects[g][q], rows).reshape(NXC, 1, 8, 128).astype(BF16)
            sx[:, g, pl.ds(lax.rem(z + q, 4), 1)] = slots
        for dx, dc, dy in SHORT_ORDER:
            px, pc = xc_at(dx, dc)
            send((z, px, pc, y_at(dy)), sx.at[px * NC + pc, g], rx.at[g, me], phase)
        rx[g, me] = sx[xc, g]

    all_of(rd.at[1:11], 8).wait_recv()
    to_experts(0, 9)
    all_of(rd.at[1:6], 12).wait_recv()
    to_experts(1, 13)

    pieces = [rd[10 - i].astype(F32)[4 * i : 4 * i + 4] for i in range(4)]
    own_rows = []
    for k in range(4):
        row = jnp.zeros((4, 128), F32)
        for i in range(4):
            row = jnp.where(lax.rem(z + 10 - i, 4) == k, pieces[i], row)
        own_rows.append(row)

    for one in loads[12:]:
        one.wait()
    all_of(rx.at[0, 1:NSHORT], 9).wait_recv()
    all_of(rx.at[1, 1:NSHORT], 13).wait_recv()
    rx_v = rx.reshape(2, NXC, NY, 4, 8, 128)
    chunks = [rx_v[:, :, k // 4, k % 4].astype(F32).reshape(128, 128) for k in range(16)]
    square = chunks[0] * chunks[0]
    for k in range(1, 16):
        square = square + chunks[k] * chunks[k]
    scale_two = lax.rsqrt(jnp.sum(square, axis=-1, keepdims=True) * (1.0 / 2048.0) + EPS)
    lhs = jnp.concatenate(
        [(chunks[k] * scale_two * mgain_ref[k : k + 1, :]).astype(BF16) for k in range(16)], axis=1
    )
    gated = dot(lhs, wg_v[...], NT)
    upped = dot(lhs, wu_v[...], NT)
    act = (gated / (1.0 + jnp.exp(-gated)) * upped).astype(BF16)
    for p in range(NY):
        down = dot(act, wd_v[:, 512 * p : 512 * p + 512])
        for k in range(4):
            se[:, :, p, k] = down[:, 128 * k : 128 * k + 128].reshape(2, NXC, 8, 128).astype(BF16)

    for g, phase in ((1, 10), (0, 14)):
        for dx, dc, dy in SHORT_ORDER:
            px, pc = xc_at(dx, dc)
            p = y_at(dy)
            send((z, px, pc, p), se.at[g, px * NC + pc, p], re.at[g, me], phase)
        re[g, me] = se[g, xc, y]

    re_v = re.reshape(2, NXC, NY, 4, 8, 128)

    def to_tokens(g):
        totals = []
        for k in range(4):
            total = re_v[g, :, 0, k].astype(F32)
            for p in range(1, NY):
                total = total + re_v[g, :, p, k].astype(F32)
            totals.append(total.reshape(64, 128).astype(BF16))
        for p in range(2):
            mixed = dot(combines[g], jnp.concatenate(totals[2 * p : 2 * p + 2], axis=0), TN)
            sf[g, :, p] = mixed.reshape(8, 8, 128).astype(BF16)
        for b in (4, 3, 5, 2, 6, 1, 7, 0) if g else (0, 7, 1, 6, 2, 5, 3, 4):
            off = (b - 4 + 8 * g) % NZ
            if off:
                send((z_at(off), x, c, y), sf.at[g, b], rf.at[NZ - off], 11)

    all_of(re.at[1, 1:NSHORT], 10).wait_recv()
    to_tokens(1)
    all_of(re.at[0, 1:NSHORT], 14).wait_recv()
    to_tokens(0)
    rf[0] = sf[0, 4]

    all_of(rf.at[1:NZ], 11).wait_recv()
    routed = jnp.sum(rf[...].astype(F32), axis=0).reshape(16, 128)
    for k in range(4):
        out_ref[:, 128 * k : 128 * k + 128] = (own_rows[k] + routed[4 * k : 4 * k + 4]).astype(BF16)

    for ref, phase in (
        (rn.at[1:NZ], 0),
        (wq_g.at[1:NXC], 1),
        (rh.at[1:4], 2),
        (rr.at[1:NZ], 3),
        (wo_r.at[1:4], 4),
        (rq.at[1:NZ], 5),
        (ro.at[1:NZ], 6),
        (wo_g.at[1:NSHORT], 7),
        (rd.at[1:11], 8),
        (rx.at[0, 1:NSHORT], 9),
        (re.at[1, 1:NSHORT], 10),
        (rf.at[1:NZ], 11),
        (rd.at[1:6], 12),
        (rx.at[1, 1:NSHORT], 13),
        (re.at[0, 1:NSHORT], 14),
    ):
        all_of(ref, phase).wait_send()


def body(
    hidden,
    attn_gain,
    query_weight,
    head_bias,
    key_cache,
    value_cache,
    lengths,
    out_weight,
    moe_gain,
    route_group,
    route_inner,
    route_weight,
    gate_w,
    up_w,
    down_w,
):
    vmem = pl.BlockSpec(memory_space=pltpu.VMEM)
    hbm = pl.BlockSpec(memory_space=pltpu.HBM)

    def buf(*shape):
        return pltpu.VMEM(shape, BF16)

    return pl.pallas_call(
        kernel,
        out_shape=jax.ShapeDtypeStruct((4, 512), BF16),
        in_specs=[hbm] * 15,
        out_specs=vmem,
        scratch_shapes=[
            buf(4, 2048),
            pltpu.VMEM((16, 128), F32),
            buf(16, 512),
            pltpu.SMEM((16,), F32),
            pltpu.SMEM((4,), jnp.int32),
            buf(16, 512),
            pltpu.VMEM((16, 128), F32),
            pltpu.SMEM((4,), jnp.int32),
            pltpu.SMEM((2, 4), jnp.int32),
            buf(2, 4),
            buf(4, 1024, 128),
            buf(4, 1024, 128),
            buf(192, 2048),
            buf(192, 2048),
            buf(192, 2048),
            buf(NXC, 16, 512),
            buf(4, 16, 512),
            buf(NSHORT, 16, 512),
            buf(NZ, 8, 128),
            buf(NZ, 8, 128),
            buf(8, 128),
            buf(NZ, 8, 128),
            buf(4, 8, 128),
            buf(NZ, 8, 128),
            buf(NZ, 2, 8, 128),
            buf(NZ, 2, 8, 128),
            buf(16, 128),
            buf(NZ, 16, 128),
            buf(16, 128),
            buf(NZ, 16, 128),
            buf(NXC, 2, 4, 8, 128),
            buf(2, NSHORT, 4, 8, 128),
            buf(2, NXC, NY, 4, 8, 128),
            buf(2, NSHORT, 4, 8, 128),
            buf(2, 8, 2, 8, 128),
            buf(NZ, 2, 8, 128),
            pltpu.SemaphoreType.DMA((15,)),
            pltpu.SemaphoreType.DMA((15,)),
            pltpu.SemaphoreType.DMA((15,)),
        ],
        compiler_params=pltpu.CompilerParams(
            collective_id=0, has_side_effects=True, vmem_limit_bytes=67043328
        ),
        name="layer",
    )(
        hidden,
        attn_gain.reshape(16, 128),
        query_weight,
        head_bias,
        key_cache.reshape(4, 1024, 128),
        value_cache.reshape(4, 1024, 128),
        lengths,
        out_weight.T,
        moe_gain.reshape(16, 128),
        route_group,
        route_inner.T,
        route_weight.T,
        jnp.swapaxes(gate_w, 1, 2).reshape(192, 2048),
        jnp.swapaxes(up_w, 1, 2).reshape(192, 2048),
        down_w.reshape(192, 2048),
    )


def solution(mesh):
    torus = Mesh(mesh.devices.reshape(NZ, NX, NC, NY), ("ep_0", "ep_1", "ep_2", "tp"))
    placed = (
        P(EP, None),
        P(),
        P(EP, "tp"),
        P(),
        P(EP, "tp", None, None),
        P(EP, "tp", None, None),
        P(EP),
        P("tp", EP),
        P(),
        P(EP),
        P(EP, None),
        P(EP, None),
        P(EP, None, "tp"),
        P(EP, None, "tp"),
        P(EP, "tp", None),
    )
    return jax.shard_map(body, mesh=torus, in_specs=placed, out_specs=P(EP, "tp"), check_vma=False)
```

time: 76.6 us -> 68.4 us (0.89)
  Pallas kernels: 75 us -> 66.8 us
    pallas_call x1, Pallas kernels: 75 us -> 66.8 us  [body(): pl.pallas_call(kernel, out_shape=jax.ShapeDtypeStruct((4, 512), BF16), in...]
where the time goes in v3:
time: 68.4 us; the launch traced here: 68.1 us
  Pallas kernels  66.8 us (98%)
  local copies, waits for them, and re-layouts  1.28 us (2%)
    pallas_call x1, Pallas kernels, body(): pl.pallas_call(kernel, out_shape=jax.ShapeDtypeStruct((4, 512), BF16), in...  66.8 us

profile of v3, /device:TPU:1, one launch (start us, length us, event | category | flops | bytes accessed | tf_op | source)
XLA Modules:
  0.0 68.1 jit_solution(2788035190288077273)
XLA Ops:
  0.0 66.8 %layer.1 = bf16[4,512]{1,0:T(4,128)(2,1)} custom-call(bf16[4,2048]{1,0:T(4,128)(2,1)} %hid_hbm.1, f32[16,128]{1,0:T(8,128)} %bitcast.20, bf16[16,512]{1,0:T(8,128)(2,1)} %wq_hbm.1, f32[16]{0:T(128)} %bias_hbm.1, bf16[4,1024,128]{2,1,0:T(8,128)(2,1)} %bitcast.14, bf16[4,1024,128]{2,1,0:T(8,128)(2,1)} %bitcast.15, s32[4]{0:T(128)} %len_hbm.1, ...), custom_call_target="tpu_custom_call" | custom-call | tf_op jit(solution)/shard_map/layer/pallas_call | solution.py:466
  66.9 1.3 %copy.17 = bf16[4,512]{1,0:T(4,128)(2,1)} copy(bf16[4,512]{1,0:T(4,128)(2,1)} %layer.1) | data formatting | bytes 8192

commit v4 on v3

--- a/solution.py
+++ b/solution.py
@@ -16,6 +16,7 @@
 EPS = 1e-06
 
 Z_ORDER = (8, 7, 9, 6, 10, 5, 11, 4, 12, 3, 13, 2, 14, 1, 15)
+NEAR_ORDER = (4, 12, 3, 13, 2, 14, 1, 15)
 HOPS = (0, 1, 2, 1)
 XC_ORDER = sorted(((dx, dc) for dx in range(NX) for dc in range(NC) if dx or dc), key=lambda d: (-HOPS[d[0]], d))
 SHORT_ORDER = sorted(
@@ -69,10 +70,12 @@
     wg_v,
     wu_v,
     wd_v,
+    wq_r,
     wq_g,
     wo_r,
     wo_g,
     sn,
+    st,
     sh,
     sr,
     rn,
@@ -115,13 +118,13 @@
     def greet(device):
         pl.semaphore_signal(barrier, inc=1, device_id=device, device_id_type=MESH)
 
-    for off in Z_ORDER:
+    for off in NEAR_ORDER:
         greet((z_at(off), x, c, y))
     for dx, dc in XC_ORDER:
         greet((z, *xc_at(dx, dc), y))
     for dy in range(1, NY):
         greet((z, x, c, y_at(dy)))
-    greeted = NZ - 1 + NXC - 1 + NY - 1
+    greeted = len(NEAR_ORDER) + NXC - 1 + NY - 1
 
     copies = (
         (hid_hbm, hid_ref),
@@ -154,6 +157,9 @@
         part = hid2[:, 128 * k : 128 * k + 128]
         sn[k] = (part * scale2 * again_ref[k : k + 1, :]).astype(BF16)
         sh[k] = part.astype(BF16)
+    first8 = iota((8, 128), 0) < 4
+    for i in range(8):
+        st[i] = jnp.where(first8, sn[z_at(i)].astype(F32), sn[z_at(i + 8)].astype(F32)).astype(BF16)
 
     lane = iota((1, 128), 1)
     tok_a = lane % 4
@@ -203,17 +209,12 @@
             device_id_type=MESH,
         )
 
-    def gather_line(src_of, dst, phase):
-        for off in Z_ORDER:
-            send((z_at(off), x, c, y), src_of(off), dst.at[NZ - off], phase)
-
-    gather_line(lambda off: sn.at[z_at(off)], rn, 0)
-    for dx, dc in XC_ORDER:
-        send((z, *xc_at(dx, dc), y), wq_ref, wq_g.at[xc], 1)
-    quad = lax.div(z, 4)
-    for off in (8, 4, 12):
-        send((z_at(off), x, c, y), wo_t, wo_r.at[quad], 4)
-    gather_line(lambda off: sr, rr, 3)
+    send((z_at(12), x, c, y), wq_ref, wq_r.at[0], 1)
+    send((z_at(4), x, c, y), wq_ref, wq_r.at[1], 12)
+    for i in (0, 1, 7, 2, 6, 3, 5):
+        send((z_at((i - 4) % NZ), x, c, y), st.at[i], rn.at[i], 0)
+    for slot, off in ((1, 12), (3, 4)):
+        send((z_at(off), x, c, y), wo_t, wo_r.at[slot], 4)
 
     def near_chunk(off):
         return lax.rem(z + off, 4) + 4 * y
@@ -222,29 +223,66 @@
         if i != 2:
             off = (2 - i) % NZ
             send((z_at(off), x, c, y), sh.at[near_chunk(off)], rh.at[i], 2)
-    rn[0] = sn[z]
+    rn[4] = st[4]
     rr[0] = sr[...]
     rh[2] = sh[near_chunk(0)]
-    wq_g[xc] = wq_ref[...]
-    wo_r[quad] = wo_t[...]
-
-    all_of(rn.at[1:NZ], 0).wait_recv()
-    all_of(wq_g.at[1:NXC], 1).wait_recv()
-
-    first = (iota((128, 128), 0) % 8) < 4
-    xin = rn[...].astype(F32).reshape(128, 128).astype(BF16)
-    part_q = dot(xin, wq_g[...].reshape(128, 512))
+    wo_r[0] = wo_t[...]
+
+    quad = lax.div(z, 4)
+
+    def gather_rows(slot, phase):
+        all_of(wq_r.at[0], phase).wait_recv()
+        for dx, dc in XC_ORDER:
+            send((z, *xc_at(dx, dc), y), wq_r.at[slot], wq_g.at[xc, slot], 15)
+
+    @pl.when(lax.rem(quad, 2) == 0)
+    def _():
+        gather_rows(0, 1)
+        gather_rows(1, 12)
+
+    @pl.when(lax.rem(quad, 2) == 1)
+    def _():
+        gather_rows(1, 12)
+        gather_rows(0, 1)
+
+    wq_g[xc] = wq_r[...]
+    all_of(wo_r.at[0:2], 4).wait_recv()
+    send((z_at(12), x, c, y), wo_r.at[1], wo_r.at[2], 16)
+    for off in Z_ORDER:
+        send((z_at(off), x, c, y), sr, rr.at[NZ - off], 3)
+    all_of(rn.at[1:8], 0).wait_recv()
+    xin = rn[...].astype(F32).reshape(64, 128).astype(BF16)
+    all_of(wq_g.at[1:NXC], 15).wait_recv()
+
+    first_q = (iota((64, 512), 0) % 8) < 4
+    part_q = jnp.where(
+        first_q, dot(xin, wq_g[:, 0].reshape(128, 512)), dot(xin, wq_g[:, 1].reshape(128, 512))
+    ).reshape(8, 8, 512)
+    part_q = (part_q + pltpu.roll(part_q, 4, 1)).reshape(64, 512)
+    first = first_q[:, 0:128]
     for p in range(2):
         pair = jnp.where(first, part_q[:, 256 * p : 256 * p + 128], part_q[:, 256 * p + 128 : 256 * p + 256])
-        sq[:, p] = pair.reshape(NZ, 8, 128).astype(BF16)
-    gather_line(lambda off: sq.at[off], rq, 5)
-    rq[0] = sq[0]
-
-    all_of(wo_r.at[1:4], 4).wait_recv()
-    for dx, dc, dy in SHORT_ORDER:
-        p = y_at(dy)
-        send((z, *xc_at(dx, dc), p), wo_r.at[p], wo_g.at[y * NXC + xc], 7)
-    wo_g[y * NXC + xc] = wo_r[y]
+        sq[:, p] = pair.reshape(8, 8, 128).astype(BF16)
+    for i in (0, 1, 7, 2, 6, 3, 5):
+        send((z_at((4 - i) % NZ), x, c, y), sq.at[i], rq.at[i], 5)
+    rq[4] = sq[4]
+
+
+    def share(slot):
+        p = lax.rem(quad + slot, NY)
+        for dx, dc in XC_ORDER:
+            send((z, *xc_at(dx, dc), p), wo_r.at[slot], wo_g.at[y * NXC + xc], 7)
+
+        @pl.when(p != y)
+        def _():
+            send((z, x, c, p), wo_r.at[slot], wo_g.at[y * NXC + xc], 7)
+
+        @pl.when(p == y)
+        def _():
+            wo_g[y * NXC + xc] = wo_r[slot]
+
+    for slot in (0, 1, 3):
+        share(slot)
 
     later = (iota((128, 128), 0) > iota((128, 128), 1)).astype(F32)
     rowh = iota((16, 1), 0)
@@ -254,7 +292,9 @@
         bias = jnp.where(rowh // 4 == h, bias_ref[4 * y + h], bias)
         length = jnp.where(rowh % 4 == h, len_ref[h], length)
 
-    all_of(rq.at[1:NZ], 5).wait_recv()
+    all_of(wo_r.at[0:1], 16).wait_recv()
+    share(2)
+    all_of(rq.at[1:8], 5).wait_recv()
     q = jnp.sum(rq[...].astype(F32), axis=0).reshape(16, 128).astype(BF16)
     loads[10].wait()
     tok = iota((16, 1024), 0) % 4
@@ -290,34 +330,6 @@
                 send((z_at((2 - i) % NZ), x, c, y_at(dy)), so, ro.at[4 * y + i], 6)
     ro[4 * y + 2] = so[...]
 
-    all_of(rr.at[1:NZ], 3).wait_recv()
-    route = jnp.sum(rr[...].astype(F32), axis=0)
-    ids = pltpu.roll(route, lax.rem(4 * (NZ + 4 - z), 128), 1)
-    wides = pltpu.roll(route, lax.rem(8 * (NZ + 4 - z), 128), 1)
-
-    def select_of(g, start, count):
-        shape = (64, 16 * count)
-        row = iota(shape, 0)
-        expert = (NXC * z + row // 8).astype(F32)
-        same = iota(shape, 1) // 4 + (start - 6) == 8 * g + row % 8
-        own = pltpu.roll(ids, (4 * (6 - start)) % 128, 1)
-        wanted = (own[0:1, 0 : 16 * count] == expert) | (own[1:2, 0 : 16 * count] == expert)
-        return jnp.where(same & wanted, 1.0, 0.0).astype(BF16)
-
-    starts = ((4, 3), (5, 3), (6, 2), (3, 3))
-    selects = [[select_of(g, start + 8 * g, count) for start, count in starts] for g in range(2)]
-
-    def combine_of(g):
-        row = iota((128, 64), 0)
-        col = iota((128, 64), 1)
-        expert = (NXC * z + (row // 8) % NXC).astype(F32)
-        same = (row % 8 == col // 8) & (row // 64 == (col // 4) % 2)
-        own = wides[:, 64 * g : 64 * g + 64]
-        weight = jnp.where(own[2:3] == expert, own[4:5], 0.0) + jnp.where(own[3:4] == expert, own[5:6], 0.0)
-        return jnp.where(same, weight, 0.0).astype(BF16)
-
-    combines = [combine_of(g) for g in range(2)]
-
     all_of(rh.at[1:4], 2).wait_recv()
     all_of(wo_g.at[1:NSHORT], 7).wait_recv()
     all_of(ro.at[1:NZ], 6).wait_recv()
@@ -332,67 +344,87 @@
         proj = jnp.sum(proj.reshape(4, 2, 8, 128), axis=1)
         proj = proj + pltpu.roll(proj, 4, 1)
         resid = resid + proj.astype(BF16).astype(F32)
-    first8 = iota((8, 128), 0) < 4
     sd[...] = jnp.concatenate(
         [jnp.where(first8, resid[0], resid[1]), jnp.where(first8, resid[2], resid[3])], axis=0
     ).astype(BF16)
 
     for off in Z_ORDER:
-        send((z_at(off), x, c, y), sd, rd.at[(8 - off) % NZ], 12 if 6 <= off <= 10 else 8)
-    rd[8] = sd[...]
+        send((z_at(off), x, c, y), sd, rd.at[z], 8)
+    rd[z] = sd[...]
+
+    all_of(rr.at[1:NZ], 3).wait_recv()
+    route = jnp.sum(rr[...].astype(F32), axis=0)
+
+    def select_of(start, count, g):
+        shape = (64, 16 * count)
+        row = iota(shape, 0)
+        expert = (NXC * z + row // 8).astype(F32)
+        same = iota(shape, 1) // 4 + (start - 2) == 8 * g + row % 8
+        own = pltpu.roll(route, (4 * (2 - start)) % 128, 1)
+        wanted = (own[0:1, 0 : 16 * count] == expert) | (own[1:2, 0 : 16 * count] == expert)
+        return jnp.where(same & wanted, 1.0, 0.0).astype(BF16)
+
+    starts = ((0, 3), (1, 3), (2, 2), (-1, 3))
+    selects = [[select_of(start + 8 * g, count, g) for start, count in starts] for g in range(2)]
+
+    def combine_of(g):
+        row = iota((128, 64), 0)
+        col = iota((128, 64), 1)
+        expert = (NXC * z + (row // 8) % NXC).astype(F32)
+        same = (row % 8 == col // 8) & (row // 64 == (col // 4) % 2)
+        own = route[:, 64 * g : 64 * g + 64]
+        weight = jnp.where(own[2:3] == expert, own[4:5], 0.0) + jnp.where(own[3:4] == expert, own[5:6], 0.0)
+        return jnp.where(same, weight, 0.0).astype(BF16)
+
+    combines = [combine_of(g) for g in range(2)]
 
     def to_experts(g, phase):
-        for q, (start, count) in enumerate(starts):
-            rows = jnp.concatenate([rd[(start + 8 * g + 4 * k) % NZ] for k in range(count)], axis=0)
-            slots = dot(selects[g][q], rows).reshape(NXC, 1, 8, 128).astype(BF16)
-            sx[:, g, pl.ds(lax.rem(z + q, 4), 1)] = slots
+        for k, (start, count) in enumerate(starts):
+            rows = jnp.concatenate([rd[(start + 8 * g + 4 * n) % NZ] for n in range(count)], axis=0)
+            sx[:, g, k] = dot(selects[g][k], rows).reshape(NXC, 8, 128).astype(BF16)
         for dx, dc, dy in SHORT_ORDER:
             px, pc = xc_at(dx, dc)
             send((z, px, pc, y_at(dy)), sx.at[px * NC + pc, g], rx.at[g, me], phase)
         rx[g, me] = sx[xc, g]
 
-    all_of(rd.at[1:11], 8).wait_recv()
+    all_of(rd.at[1:NZ], 8).wait_recv()
     to_experts(0, 9)
-    all_of(rd.at[1:6], 12).wait_recv()
     to_experts(1, 13)
 
-    pieces = [rd[10 - i].astype(F32)[4 * i : 4 * i + 4] for i in range(4)]
+    pieces = [rd[z_at(18 - i)].astype(F32)[4 * i : 4 * i + 4] for i in range(4)]
     own_rows = []
     for k in range(4):
         row = jnp.zeros((4, 128), F32)
         for i in range(4):
-            row = jnp.where(lax.rem(z + 10 - i, 4) == k, pieces[i], row)
+            row = jnp.where(lax.rem(z + 18 - i, 4) == k, pieces[i], row)
         own_rows.append(row)
 
-    for one in loads[12:]:
-        one.wait()
-    all_of(rx.at[0, 1:NSHORT], 9).wait_recv()
-    all_of(rx.at[1, 1:NSHORT], 13).wait_recv()
     rx_v = rx.reshape(2, NXC, NY, 4, 8, 128)
-    chunks = [rx_v[:, :, k // 4, k % 4].astype(F32).reshape(128, 128) for k in range(16)]
-    square = chunks[0] * chunks[0]
-    for k in range(1, 16):
-        square = square + chunks[k] * chunks[k]
-    scale_two = lax.rsqrt(jnp.sum(square, axis=-1, keepdims=True) * (1.0 / 2048.0) + EPS)
-    lhs = jnp.concatenate(
-        [(chunks[k] * scale_two * mgain_ref[k : k + 1, :]).astype(BF16) for k in range(16)], axis=1
-    )
-    gated = dot(lhs, wg_v[...], NT)
-    upped = dot(lhs, wu_v[...], NT)
-    act = (gated / (1.0 + jnp.exp(-gated)) * upped).astype(BF16)
-    for p in range(NY):
-        down = dot(act, wd_v[:, 512 * p : 512 * p + 512])
-        for k in range(4):
-            se[:, :, p, k] = down[:, 128 * k : 128 * k + 128].reshape(2, NXC, 8, 128).astype(BF16)
-
-    for g, phase in ((1, 10), (0, 14)):
+    re_v = re.reshape(2, NXC, NY, 4, 8, 128)
+
+    def experts(g, phase):
+        chunks = [rx_v[g, :, k // 4, k % 4].astype(F32).reshape(64, 128) for k in range(16)]
+        square = chunks[0] * chunks[0]
+        for k in range(1, 16):
+            square = square + chunks[k] * chunks[k]
+        scale_two = lax.rsqrt(jnp.sum(square, axis=-1, keepdims=True) * (1.0 / 2048.0) + EPS)
+        lhs = jnp.concatenate(
+            [(chunks[k] * scale_two * mgain_ref[k : k + 1, :]).astype(BF16) for k in range(16)], axis=1
+        )
+        gated = dot(lhs, wg_v[...], NT)
+        upped = dot(lhs, wu_v[...], NT)
+        act = (gated / (1.0 + jnp.exp(-gated)) * upped).astype(BF16)
+        for p in range(NY):
+            down = dot(act, wd_v[:, 512 * p : 512 * p + 512])
+            for k in range(4):
+                se[g, :, p, k] = down[:, 128 * k : 128 * k + 128].reshape(NXC, 8, 128).astype(BF16)
         for dx, dc, dy in SHORT_ORDER:
             px, pc = xc_at(dx, dc)
             p = y_at(dy)
             send((z, px, pc, p), se.at[g, px * NC + pc, p], re.at[g, me], phase)
         re[g, me] = se[g, xc, y]
 
-    re_v = re.reshape(2, NXC, NY, 4, 8, 128)
+    half = lax.div(z, 8)
 
     def to_tokens(g):
         totals = []
@@ -404,16 +436,29 @@
         for p in range(2):
             mixed = dot(combines[g], jnp.concatenate(totals[2 * p : 2 * p + 2], axis=0), TN)
             sf[g, :, p] = mixed.reshape(8, 8, 128).astype(BF16)
-        for b in (4, 3, 5, 2, 6, 1, 7, 0) if g else (0, 7, 1, 6, 2, 5, 3, 4):
-            off = (b - 4 + 8 * g) % NZ
-            if off:
-                send((z_at(off), x, c, y), sf.at[g, b], rf.at[NZ - off], 11)
-
-    all_of(re.at[1, 1:NSHORT], 10).wait_recv()
+
+        def back(j):
+            b = lax.rem(z + j, 8)
+            send((8 * g + b, x, c, y), sf.at[g, b], rf.at[z], 11)
+
+        @pl.when(half != g)
+        def _():
+            back(0)
+
+        for j in (4, 3, 5, 2, 6, 1, 7):
+            back(j)
+
+    for one in loads[12:]:
+        one.wait()
+    all_of(rx.at[0, 1:NSHORT], 9).wait_recv()
+    experts(0, 10)
+    all_of(rx.at[1, 1:NSHORT], 13).wait_recv()
+    experts(1, 14)
+    all_of(re.at[0, 1:NSHORT], 10).wait_recv()
+    to_tokens(0)
+    all_of(re.at[1, 1:NSHORT], 14).wait_recv()
     to_tokens(1)
-    all_of(re.at[0, 1:NSHORT], 14).wait_recv()
-    to_tokens(0)
-    rf[0] = sf[0, 4]
+    rf[z] = sf[half, lax.rem(z, 8)]
 
     all_of(rf.at[1:NZ], 11).wait_recv()
     routed = jnp.sum(rf[...].astype(F32), axis=0).reshape(16, 128)
@@ -421,21 +466,23 @@
         out_ref[:, 128 * k : 128 * k + 128] = (own_rows[k] + routed[4 * k : 4 * k + 4]).astype(BF16)
 
     for ref, phase in (
-        (rn.at[1:NZ], 0),
-        (wq_g.at[1:NXC], 1),
+        (rn.at[1:8], 0),
+        (wq_r.at[0], 1),
+        (wq_r.at[0], 12),
         (rh.at[1:4], 2),
         (rr.at[1:NZ], 3),
-        (wo_r.at[1:4], 4),
-        (rq.at[1:NZ], 5),
+        (wo_r.at[0:2], 4),
+        (rq.at[1:8], 5),
         (ro.at[1:NZ], 6),
         (wo_g.at[1:NSHORT], 7),
-        (rd.at[1:11], 8),
+        (rd.at[1:NZ], 8),
         (rx.at[0, 1:NSHORT], 9),
-        (re.at[1, 1:NSHORT], 10),
+        (re.at[0, 1:NSHORT], 10),
         (rf.at[1:NZ], 11),
-        (rd.at[1:6], 12),
         (rx.at[1, 1:NSHORT], 13),
-        (re.at[0, 1:NSHORT], 14),
+        (re.at[1, 1:NSHORT], 14),
+        (wq_g.at[1:NXC], 15),
+        (wo_r.at[0:1], 16),
     ):
         all_of(ref, phase).wait_send()
 
@@ -484,17 +531,19 @@
             buf(192, 2048),
             buf(192, 2048),
             buf(192, 2048),
-            buf(NXC, 16, 512),
+            buf(2, 16, 512),
+            buf(NXC, 2, 16, 512),
             buf(4, 16, 512),
             buf(NSHORT, 16, 512),
             buf(NZ, 8, 128),
+            buf(8, 8, 128),
             buf(NZ, 8, 128),
             buf(8, 128),
-            buf(NZ, 8, 128),
+            buf(8, 8, 128),
             buf(4, 8, 128),
             buf(NZ, 8, 128),
-            buf(NZ, 2, 8, 128),
-            buf(NZ, 2, 8, 128),
+            buf(8, 2, 8, 128),
+            buf(8, 2, 8, 128),
             buf(16, 128),
             buf(NZ, 16, 128),
             buf(16, 128),
@@ -506,8 +555,8 @@
             buf(2, 8, 2, 8, 128),
             buf(NZ, 2, 8, 128),
             pltpu.SemaphoreType.DMA((15,)),
-            pltpu.SemaphoreType.DMA((15,)),
-            pltpu.SemaphoreType.DMA((15,)),
+            pltpu.SemaphoreType.DMA((17,)),
+            pltpu.SemaphoreType.DMA((17,)),
         ],
         compiler_params=pltpu.CompilerParams(
             collective_id=0, has_side_effects=True, vmem_limit_bytes=67043328

time: 68.4 us -> 66.1 us (0.966)
  Pallas kernels: 66.8 us -> 64.5 us
    pallas_call x1, Pallas kernels: 66.8 us -> 64.5 us  [body(): pl.pallas_call(kernel, out_shape=jax.ShapeDtypeStruct((4, 512), BF16), in...]
where the time goes in v4:
time: 66.1 us; the launch traced here: 65.8 us
  Pallas kernels  64.5 us (98%)
  local copies, waits for them, and re-layouts  1.28 us (2%)
    pallas_call x1, Pallas kernels, body(): pl.pallas_call(kernel, out_shape=jax.ShapeDtypeStruct((4, 512), BF16), in...  64.5 us

profile of v4, /device:TPU:1, one launch (start us, length us, event | category | flops | bytes accessed | tf_op | source)
XLA Modules:
  0.0 65.8 jit_solution(11034499657203878883)
XLA Ops:
  0.0 64.5 %layer.1 = bf16[4,512]{1,0:T(4,128)(2,1)} custom-call(bf16[4,2048]{1,0:T(4,128)(2,1)} %hid_hbm.1, f32[16,128]{1,0:T(8,128)} %bitcast.20, bf16[16,512]{1,0:T(8,128)(2,1)} %wq_hbm.1, f32[16]{0:T(128)} %bias_hbm.1, bf16[4,1024,128]{2,1,0:T(8,128)(2,1)} %bitcast.14, bf16[4,1024,128]{2,1,0:T(8,128)(2,1)} %bitcast.15, s32[4]{0:T(128)} %len_hbm.1, ...), custom_call_target="tpu_custom_call" | custom-call | tf_op jit(solution)/shard_map/layer/pallas_call | solution.py:513
  64.6 1.3 %copy.17 = bf16[4,512]{1,0:T(4,128)(2,1)} copy(bf16[4,512]{1,0:T(4,128)(2,1)} %layer.1) | data formatting | bytes 8192

commit v5 on v4

--- a/solution.py
+++ b/solution.py
@@ -87,6 +87,10 @@
     ro,
     sd,
     rd,
+    sx4,
+    rx4,
+    se4,
+    re4,
     sx,
     rx,
     se,
@@ -96,6 +100,7 @@
     load_sem,
     send_sem,
     recv_sem,
+    past_sem,
 ):
     z = lax.axis_index("ep_0")
     x = lax.axis_index("ep_1")
@@ -209,6 +214,22 @@
             device_id_type=MESH,
         )
 
+    quad = lax.div(z, 4)
+
+    def share(slot):
+        source = wo_r.at[slot] if slot else wo_t
+        p = lax.rem(quad + slot, NY)
+        for dx, dc in XC_ORDER:
+            send((z, *xc_at(dx, dc), p), source, wo_g.at[y * NXC + xc], 7)
+
+        @pl.when(p != y)
+        def _():
+            send((z, x, c, p), source, wo_g.at[y * NXC + xc], 7)
+
+        @pl.when(p == y)
+        def _():
+            wo_g[y * NXC + xc] = source[...]
+
     send((z_at(12), x, c, y), wq_ref, wq_r.at[0], 1)
     send((z_at(4), x, c, y), wq_ref, wq_r.at[1], 12)
     for i in (0, 1, 7, 2, 6, 3, 5):
@@ -226,9 +247,8 @@
     rn[4] = st[4]
     rr[0] = sr[...]
     rh[2] = sh[near_chunk(0)]
-    wo_r[0] = wo_t[...]
-
-    quad = lax.div(z, 4)
+    for dx, dc in XC_ORDER:
+        pl.semaphore_signal(past_sem, inc=1, device_id=(z, *xc_at(dx, dc), y), device_id_type=MESH)
 
     def gather_rows(slot, phase):
         all_of(wq_r.at[0], phase).wait_recv()
@@ -250,6 +270,9 @@
     send((z_at(12), x, c, y), wo_r.at[1], wo_r.at[2], 16)
     for off in Z_ORDER:
         send((z_at(off), x, c, y), sr, rr.at[NZ - off], 3)
+    pl.semaphore_wait(past_sem, NXC - 1)
+    for slot in (0, 1, 3):
+        share(slot)
     all_of(rn.at[1:8], 0).wait_recv()
     xin = rn[...].astype(F32).reshape(64, 128).astype(BF16)
     all_of(wq_g.at[1:NXC], 15).wait_recv()
@@ -267,22 +290,6 @@
         send((z_at((4 - i) % NZ), x, c, y), sq.at[i], rq.at[i], 5)
     rq[4] = sq[4]
 
-
-    def share(slot):
-        p = lax.rem(quad + slot, NY)
-        for dx, dc in XC_ORDER:
-            send((z, *xc_at(dx, dc), p), wo_r.at[slot], wo_g.at[y * NXC + xc], 7)
-
-        @pl.when(p != y)
-        def _():
-            send((z, x, c, p), wo_r.at[slot], wo_g.at[y * NXC + xc], 7)
-
-        @pl.when(p == y)
-        def _():
-            wo_g[y * NXC + xc] = wo_r[slot]
-
-    for slot in (0, 1, 3):
-        share(slot)
 
     later = (iota((128, 128), 0) > iota((128, 128), 1)).astype(F32)
     rowh = iota((16, 1), 0)
@@ -355,41 +362,65 @@
     all_of(rr.at[1:NZ], 3).wait_recv()
     route = jnp.sum(rr[...].astype(F32), axis=0)
 
-    def select_of(start, count, g):
+    groups = ((0, 4), (4, 4), (8, 8))
+
+    def select_of(start, count, base, size):
         shape = (64, 16 * count)
         row = iota(shape, 0)
         expert = (NXC * z + row // 8).astype(F32)
-        same = iota(shape, 1) // 4 + (start - 2) == 8 * g + row % 8
+        same = iota(shape, 1) // 4 + (start - 2) == base + row % size
         own = pltpu.roll(route, (4 * (2 - start)) % 128, 1)
         wanted = (own[0:1, 0 : 16 * count] == expert) | (own[1:2, 0 : 16 * count] == expert)
         return jnp.where(same & wanted, 1.0, 0.0).astype(BF16)
 
-    starts = ((0, 3), (1, 3), (2, 2), (-1, 3))
-    selects = [[select_of(start + 8 * g, count, g) for start, count in starts] for g in range(2)]
-
-    def combine_of(g):
-        row = iota((128, 64), 0)
-        col = iota((128, 64), 1)
-        expert = (NXC * z + (row // 8) % NXC).astype(F32)
-        same = (row % 8 == col // 8) & (row // 64 == (col // 4) % 2)
-        own = route[:, 64 * g : 64 * g + 64]
+    def holders(base, size):
+        counts = (3, 3, 2, 3) if size == 8 else (2, 2, 1, 2)
+        return tuple((base + off, count) for off, count in zip((0, 1, 2, -1), counts))
+
+    selects = [[select_of(*one, base, size) for one in holders(base, size)] for base, size in groups]
+
+    def combine_of(base, size):
+        rows, cols = (128, 64) if size == 8 else (64, 32)
+        row = iota((rows, cols), 0)
+        col = iota((rows, cols), 1)
+        own = route[:, 8 * base : 8 * base + cols]
+        if size == 8:
+            expert, chunk, block = (row // 8) % NXC, row // 64, row % 8
+        else:
+            expert, chunk, block = row // 8, (row // 4) % 2, row % 4
+        expert = (NXC * z + expert).astype(F32)
+        same = (block == col // 8) & (chunk == (col // 4) % 2)
         weight = jnp.where(own[2:3] == expert, own[4:5], 0.0) + jnp.where(own[3:4] == expert, own[5:6], 0.0)
         return jnp.where(same, weight, 0.0).astype(BF16)
 
-    combines = [combine_of(g) for g in range(2)]
-
-    def to_experts(g, phase):
-        for k, (start, count) in enumerate(starts):
-            rows = jnp.concatenate([rd[(start + 8 * g + 4 * n) % NZ] for n in range(count)], axis=0)
-            sx[:, g, k] = dot(selects[g][k], rows).reshape(NXC, 8, 128).astype(BF16)
+    combines = [combine_of(base, size) for base, size in groups]
+    first64 = (iota((64, 128), 0) % 8) < 4
+    first_ff = (iota((64, 192), 0) % 8) < 4
+    bufs = ((sx4.at[0], rx4.at[0], se4.at[0], re4.at[0]), (sx4.at[1], rx4.at[1], se4.at[1], re4.at[1]), (sx, rx, se, re))
+
+    def swap(v):
+        return pltpu.roll(v.reshape(8, 8, v.shape[1]), 4, 1).reshape(v.shape)
+
+    def to_experts(n, phase):
+        out, into = bufs[n][0], bufs[n][1]
+        base, size = groups[n]
+        slots = []
+        for k, (start, count) in enumerate(holders(base, size)):
+            rows = jnp.concatenate([rd[(start + 4 * i) % NZ] for i in range(count)], axis=0)
+            slots.append(dot(selects[n][k], rows))
+        if size == 4:
+            slots = [jnp.where(first64, slots[0], slots[1]), jnp.where(first64, slots[2], slots[3])]
+        for k, slot in enumerate(slots):
+            out[:, k] = slot.reshape(NXC, 8, 128).astype(BF16)
         for dx, dc, dy in SHORT_ORDER:
             px, pc = xc_at(dx, dc)
-            send((z, px, pc, y_at(dy)), sx.at[px * NC + pc, g], rx.at[g, me], phase)
-        rx[g, me] = sx[xc, g]
+            send((z, px, pc, y_at(dy)), out.at[px * NC + pc], into.at[me], phase)
+        into[me] = out[xc]
 
     all_of(rd.at[1:NZ], 8).wait_recv()
     to_experts(0, 9)
-    to_experts(1, 13)
+    to_experts(1, 17)
+    to_experts(2, 13)
 
     pieces = [rd[z_at(18 - i)].astype(F32)[4 * i : 4 * i + 4] for i in range(4)]
     own_rows = []
@@ -399,66 +430,93 @@
             row = jnp.where(lax.rem(z + 18 - i, 4) == k, pieces[i], row)
         own_rows.append(row)
 
-    rx_v = rx.reshape(2, NXC, NY, 4, 8, 128)
-    re_v = re.reshape(2, NXC, NY, 4, 8, 128)
-
-    def experts(g, phase):
-        chunks = [rx_v[g, :, k // 4, k % 4].astype(F32).reshape(64, 128) for k in range(16)]
+    def experts(n, phase):
+        _, into, out, back = bufs[n]
+        small = groups[n][1] == 4
+        tiles = 2 if small else 4
+        slots = into.reshape(NXC, NY, tiles, 8, 128)
+        chunks = [slots[:, k // tiles, k % tiles].astype(F32).reshape(64, 128) for k in range(NY * tiles)]
         square = chunks[0] * chunks[0]
-        for k in range(1, 16):
-            square = square + chunks[k] * chunks[k]
+        for chunk in chunks[1:]:
+            square = square + chunk * chunk
+        if small:
+            square = square + swap(square)
         scale_two = lax.rsqrt(jnp.sum(square, axis=-1, keepdims=True) * (1.0 / 2048.0) + EPS)
-        lhs = jnp.concatenate(
-            [(chunks[k] * scale_two * mgain_ref[k : k + 1, :]).astype(BF16) for k in range(16)], axis=1
-        )
-        gated = dot(lhs, wg_v[...], NT)
-        upped = dot(lhs, wu_v[...], NT)
+
+        def gain(k):
+            if small:
+                return jnp.where(first64, mgain_ref[2 * k : 2 * k + 1, :], mgain_ref[2 * k + 1 : 2 * k + 2, :])
+            return mgain_ref[k : k + 1, :]
+
+        lhs = jnp.concatenate([(one * scale_two * gain(k)).astype(BF16) for k, one in enumerate(chunks)], axis=1)
+
+        def product(w):
+            if not small:
+                return dot(lhs, w[...], NT)
+            even, odd = [
+                dot(lhs, jnp.concatenate([w[:, 256 * k + o : 256 * k + o + 128] for k in range(8)], axis=1), NT)
+                for o in (0, 128)
+            ]
+            both = jnp.where(first_ff, even, odd)
+            return both + swap(both)
+
+        gated = product(wg_v)
+        upped = product(wu_v)
         act = (gated / (1.0 + jnp.exp(-gated)) * upped).astype(BF16)
         for p in range(NY):
             down = dot(act, wd_v[:, 512 * p : 512 * p + 512])
-            for k in range(4):
-                se[g, :, p, k] = down[:, 128 * k : 128 * k + 128].reshape(NXC, 8, 128).astype(BF16)
+            parts = [down[:, 128 * k : 128 * k + 128] for k in range(4)]
+            if small:
+                parts = [jnp.where(first64, parts[0], parts[1]), jnp.where(first64, parts[2], parts[3])]
+            for k, part in enumerate(parts):
+                out[:, p, k] = part.reshape(NXC, 8, 128).astype(BF16)
         for dx, dc, dy in SHORT_ORDER:
             px, pc = xc_at(dx, dc)
             p = y_at(dy)
-            send((z, px, pc, p), se.at[g, px * NC + pc, p], re.at[g, me], phase)
-        re[g, me] = se[g, xc, y]
-
-    half = lax.div(z, 8)
-
-    def to_tokens(g):
+            send((z, px, pc, p), out.at[px * NC + pc, p], back.at[me], phase)
+        back[me] = out[xc, y]
+
+    def to_tokens(n):
+        base, size = groups[n]
+        tiles = 2 if size == 4 else 4
+        parts = bufs[n][3].reshape(NXC, NY, tiles, 8, 128)
         totals = []
-        for k in range(4):
-            total = re_v[g, :, 0, k].astype(F32)
+        for k in range(tiles):
+            total = parts[:, 0, k].astype(F32)
             for p in range(1, NY):
-                total = total + re_v[g, :, p, k].astype(F32)
+                total = total + parts[:, p, k].astype(F32)
             totals.append(total.reshape(64, 128).astype(BF16))
+        if size == 8:
+            totals = [jnp.concatenate(totals[2 * p : 2 * p + 2], axis=0) for p in range(2)]
         for p in range(2):
-            mixed = dot(combines[g], jnp.concatenate(totals[2 * p : 2 * p + 2], axis=0), TN)
-            sf[g, :, p] = mixed.reshape(8, 8, 128).astype(BF16)
+            sf[base : base + size, p] = dot(combines[n], totals[p], TN).reshape(size, 8, 128).astype(BF16)
 
         def back(j):
-            b = lax.rem(z + j, 8)
-            send((8 * g + b, x, c, y), sf.at[g, b], rf.at[z], 11)
-
-        @pl.when(half != g)
+            b = base + lax.rem(z + j, size)
+            send((b, x, c, y), sf.at[b], rf.at[z], 11)
+
+        @pl.when(lax.div(z, size) != base // size)
         def _():
             back(0)
 
-        for j in (4, 3, 5, 2, 6, 1, 7):
+        for j in range(1, size):
             back(j)
 
     for one in loads[12:]:
         one.wait()
-    all_of(rx.at[0, 1:NSHORT], 9).wait_recv()
+    all_of(rx4.at[0, 1:NSHORT], 9).wait_recv()
     experts(0, 10)
-    all_of(rx.at[1, 1:NSHORT], 13).wait_recv()
-    experts(1, 14)
-    all_of(re.at[0, 1:NSHORT], 10).wait_recv()
+    all_of(rx4.at[1, 1:NSHORT], 17).wait_recv()
+    experts(1, 18)
+    all_of(rx.at[1:NSHORT], 13).wait_recv()
+    experts(2, 14)
+    all_of(re4.at[0, 1:NSHORT], 10).wait_recv()
     to_tokens(0)
-    all_of(re.at[1, 1:NSHORT], 14).wait_recv()
+    all_of(re4.at[1, 1:NSHORT], 18).wait_recv()
     to_tokens(1)
-    rf[z] = sf[half, lax.rem(z, 8)]
+    all_of(re.at[1:NSHORT], 14).wait_recv()
+    to_tokens(2)
+    rf[z] = sf[z]
 
     all_of(rf.at[1:NZ], 11).wait_recv()
     routed = jnp.sum(rf[...].astype(F32), axis=0).reshape(16, 128)
@@ -476,11 +534,13 @@
         (ro.at[1:NZ], 6),
         (wo_g.at[1:NSHORT], 7),
         (rd.at[1:NZ], 8),
-        (rx.at[0, 1:NSHORT], 9),
-        (re.at[0, 1:NSHORT], 10),
+        (rx4.at[0, 1:NSHORT], 9),
+        (rx4.at[1, 1:NSHORT], 17),
+        (re4.at[1, 1:NSHORT], 18),
+        (re4.at[0, 1:NSHORT], 10),
         (rf.at[1:NZ], 11),
-        (rx.at[1, 1:NSHORT], 13),
-        (re.at[1, 1:NSHORT], 14),
+        (rx.at[1:NSHORT], 13),
+        (re.at[1:NSHORT], 14),
         (wq_g.at[1:NXC], 15),
         (wo_r.at[0:1], 16),
     ):
@@ -548,15 +608,20 @@
             buf(NZ, 16, 128),
             buf(16, 128),
             buf(NZ, 16, 128),
-            buf(NXC, 2, 4, 8, 128),
-            buf(2, NSHORT, 4, 8, 128),
-            buf(2, NXC, NY, 4, 8, 128),
-            buf(2, NSHORT, 4, 8, 128),
-            buf(2, 8, 2, 8, 128),
+            buf(2, NXC, 2, 8, 128),
+            buf(2, NSHORT, 2, 8, 128),
+            buf(2, NXC, NY, 2, 8, 128),
+            buf(2, NSHORT, 2, 8, 128),
+            buf(NXC, 4, 8, 128),
+            buf(NSHORT, 4, 8, 128),
+            buf(NXC, NY, 4, 8, 128),
+            buf(NSHORT, 4, 8, 128),
+            buf(NZ, 2, 8, 128),
             buf(NZ, 2, 8, 128),
             pltpu.SemaphoreType.DMA((15,)),
-            pltpu.SemaphoreType.DMA((17,)),
-            pltpu.SemaphoreType.DMA((17,)),
+            pltpu.SemaphoreType.DMA((19,)),
+            pltpu.SemaphoreType.DMA((19,)),
+            pltpu.SemaphoreType.REGULAR,
         ],
         compiler_params=pltpu.CompilerParams(
             collective_id=0, has_side_effects=True, vmem_limit_bytes=67043328

time: 66.1 us -> 64.1 us (0.970)
  Pallas kernels: 64.5 us -> 62.6 us
    pallas_call x1, Pallas kernels: 64.5 us -> 62.6 us  [body(): pl.pallas_call(kernel, out_shape=jax.ShapeDtypeStruct((4, 512), BF16), in...]
where the time goes in v5:
time: 64.1 us; the launch traced here: 63.9 us
  Pallas kernels  62.6 us (98%)
  local copies, waits for them, and re-layouts  1.28 us (2%)
    pallas_call x1, Pallas kernels, body(): pl.pallas_call(kernel, out_shape=jax.ShapeDtypeStruct((4, 512), BF16), in...  62.6 us

profile of v5, /device:TPU:1, one launch (start us, length us, event | category | flops | bytes accessed | tf_op | source)
XLA Modules:
  0.0 63.9 jit_solution(3400035149504055926)
XLA Ops:
  0.0 62.6 %layer.1 = bf16[4,512]{1,0:T(4,128)(2,1)} custom-call(bf16[4,2048]{1,0:T(4,128)(2,1)} %hid_hbm.1, f32[16,128]{1,0:T(8,128)} %bitcast.20, bf16[16,512]{1,0:T(8,128)(2,1)} %wq_hbm.1, f32[16]{0:T(128)} %bias_hbm.1, bf16[4,1024,128]{2,1,0:T(8,128)(2,1)} %bitcast.14, bf16[4,1024,128]{2,1,0:T(8,128)(2,1)} %bitcast.15, s32[4]{0:T(128)} %len_hbm.1, ...), custom_call_target="tpu_custom_call" | custom-call | tf_op jit(solution)/shard_map/layer/pallas_call | solution.py:573
  62.6 1.3 %copy.17 = bf16[4,512]{1,0:T(4,128)(2,1)} copy(bf16[4,512]{1,0:T(4,128)(2,1)} %layer.1) | data formatting | bytes 8192

commit v6 on v5

--- a/solution.py
+++ b/solution.py
@@ -250,6 +250,8 @@
     for dx, dc in XC_ORDER:
         pl.semaphore_signal(past_sem, inc=1, device_id=(z, *xc_at(dx, dc), y), device_id_type=MESH)
 
+    pl.semaphore_wait(past_sem, NXC - 1)
+    share(0)
     def gather_rows(slot, phase):
         all_of(wq_r.at[0], phase).wait_recv()
         for dx, dc in XC_ORDER:
@@ -270,9 +272,6 @@
     send((z_at(12), x, c, y), wo_r.at[1], wo_r.at[2], 16)
     for off in Z_ORDER:
         send((z_at(off), x, c, y), sr, rr.at[NZ - off], 3)
-    pl.semaphore_wait(past_sem, NXC - 1)
-    for slot in (0, 1, 3):
-        share(slot)
     all_of(rn.at[1:8], 0).wait_recv()
     xin = rn[...].astype(F32).reshape(64, 128).astype(BF16)
     all_of(wq_g.at[1:NXC], 15).wait_recv()
@@ -289,6 +288,9 @@
     for i in (0, 1, 7, 2, 6, 3, 5):
         send((z_at((4 - i) % NZ), x, c, y), sq.at[i], rq.at[i], 5)
     rq[4] = sq[4]
+
+    share(1)
+    share(3)
 
 
     later = (iota((128, 128), 0) > iota((128, 128), 1)).astype(F32)
@@ -572,7 +574,7 @@
 
     return pl.pallas_call(
         kernel,
-        out_shape=jax.ShapeDtypeStruct((4, 512), BF16),
+        out_shape=pltpu.VMEM((4, 512), BF16),
         in_specs=[hbm] * 15,
         out_specs=vmem,
         scratch_shapes=[
@@ -624,10 +626,10 @@
             pltpu.SemaphoreType.REGULAR,
         ],
         compiler_params=pltpu.CompilerParams(
-            collective_id=0, has_side_effects=True, vmem_limit_bytes=67043328
+            collective_id=0, has_side_effects=True, vmem_limit_bytes=40 * 1024 * 1024
         ),
         name="layer",
-    )(
+    )(*[pltpu.with_memory_space_constraint(a, pltpu.HBM) for a in (
         hidden,
         attn_gain.reshape(16, 128),
         query_weight,
@@ -643,7 +645,7 @@
         jnp.swapaxes(gate_w, 1, 2).reshape(192, 2048),
         jnp.swapaxes(up_w, 1, 2).reshape(192, 2048),
         down_w.reshape(192, 2048),
-    )
+    )])
 
 
 def solution(mesh):

time: 64.1 us -> 62.1 us (0.969)
  Pallas kernels: 62.6 us -> 61.3 us
  local copies, waits for them, and re-layouts: 1.28 us -> 0.6 us
    pallas_call x1, Pallas kernels: 62.6 us -> 61.3 us  [body(): pl.pallas_call(kernel, out_shape=pltpu.VMEM((4, 512), BF16), in_specs=[hb...]
    unnamed x1, local copies, waits for them, and re-layouts: 1.28 us -> 0.6 us
where the time goes in v6:
time: 62.1 us; the launch traced here: 61.9 us
  Pallas kernels  61.3 us (99%)
    pallas_call x1, Pallas kernels, body(): pl.pallas_call(kernel, out_shape=pltpu.VMEM((4, 512), BF16), in_specs=[hb...  61.3 us

profile of v6, /device:TPU:1, one launch (start us, length us, event | category | flops | bytes accessed | tf_op | source)
XLA Modules:
  0.0 61.9 jit_solution(10577791850921483790)
XLA Ops:
  0.0 61.3 %layer.1 = bf16[4,512]{1,0:T(4,128)(2,1)S(1)} custom-call(bf16[4,2048]{1,0:T(4,128)(2,1)} %hid_hbm.1, f32[16,128]{1,0:T(8,128)} %bitcast.20, bf16[16,512]{1,0:T(8,128)(2,1)} %wq_hbm.1, f32[16]{0:T(128)} %bias_hbm.1, bf16[4,1024,128]{2,1,0:T(8,128)(2,1)} %bitcast.14, bf16[4,1024,128]{2,1,0:T(8,128)(2,1)} %bitcast.15, s32[4]{0:T(128)} %len_hbm.1, ...), custom_call_target="tpu_custom_call" | custom-call | tf_op jit(solution)/shard_map/layer/pallas_call | solution.py:575
  61.3 0.6 copy.17

commit v7 on v6

--- a/solution.py
+++ b/solution.py
@@ -21,7 +21,7 @@
 XC_ORDER = sorted(((dx, dc) for dx in range(NX) for dc in range(NC) if dx or dc), key=lambda d: (-HOPS[d[0]], d))
 SHORT_ORDER = sorted(
     ((dx, dc, dy) for dx in range(NX) for dc in range(NC) for dy in range(NY) if dx or dc or dy),
-    key=lambda d: (-HOPS[d[0]] - HOPS[d[2]], d),
+    key=lambda d: (-HOPS[d[0]] - HOPS[d[2]], d[1], d[0] % 2, d),
 )
 
 NT = (((1,), (1,)), ((), ()))
@@ -293,7 +293,7 @@
     share(3)
 
 
-    later = (iota((128, 128), 0) > iota((128, 128), 1)).astype(F32)
+    later = (iota((128, 128), 0) > iota((128, 128), 1)).astype(BF16)
     rowh = iota((16, 1), 0)
     bias = jnp.zeros((16, 1), F32)
     length = jnp.zeros((16, 1), jnp.int32)
@@ -316,7 +316,10 @@
     visible = iota((16, 1024), 1) < length
     log_keep = jnp.where(visible, log_stop - scores, 0.0)
     stacked = jnp.concatenate([log_keep[:, 128 * k : 128 * k + 128] for k in range(8)], axis=0)
-    within = dot(stacked, later, precision=lax.Precision.HIGHEST)
+    high = stacked.astype(BF16)
+    mid = (stacked - high.astype(F32)).astype(BF16)
+    low = (stacked - high.astype(F32) - mid.astype(F32)).astype(BF16)
+    within = dot(high, later) + dot(mid, later) + dot(low, later)
     carry_sum = jnp.zeros((16, 1), F32)
     weights = [None] * 8
     for k in reversed(range(8)):
@@ -450,7 +453,7 @@
                 return jnp.where(first64, mgain_ref[2 * k : 2 * k + 1, :], mgain_ref[2 * k + 1 : 2 * k + 2, :])
             return mgain_ref[k : k + 1, :]
 
-        lhs = jnp.concatenate([(one * scale_two * gain(k)).astype(BF16) for k, one in enumerate(chunks)], axis=1)
+        lhs = jnp.concatenate([(one * gain(k)).astype(BF16) for k, one in enumerate(chunks)], axis=1)
 
         def product(w):
             if not small:
@@ -462,8 +465,8 @@
             both = jnp.where(first_ff, even, odd)
             return both + swap(both)
 
-        gated = product(wg_v)
-        upped = product(wu_v)
+        gated = product(wg_v) * scale_two
+        upped = product(wu_v) * scale_two
         act = (gated / (1.0 + jnp.exp(-gated)) * upped).astype(BF16)
         for p in range(NY):
             down = dot(act, wd_v[:, 512 * p : 512 * p + 512])

time: 62.1 us -> 62.1 us (level)
  no operation moved by 1% of the time
where the time goes in v7:
time: 62.1 us; the launch traced here: 61.8 us
  Pallas kernels  61.2 us (99%)
    pallas_call x1, Pallas kernels, body(): pl.pallas_call(kernel, out_shape=pltpu.VMEM((4, 512), BF16), in_specs=[hb...  61.2 us

profile of v7, /device:TPU:1, one launch (start us, length us, event | category | flops | bytes accessed | tf_op | source)
XLA Modules:
  0.0 61.8 jit_solution(4619967262767543711)
XLA Ops:
  0.0 61.2 %layer.1 = bf16[4,512]{1,0:T(4,128)(2,1)S(1)} custom-call(bf16[4,2048]{1,0:T(4,128)(2,1)} %hid_hbm.1, f32[16,128]{1,0:T(8,128)} %bitcast.20, bf16[16,512]{1,0:T(8,128)(2,1)} %wq_hbm.1, f32[16]{0:T(128)} %bias_hbm.1, bf16[4,1024,128]{2,1,0:T(8,128)(2,1)} %bitcast.14, bf16[4,1024,128]{2,1,0:T(8,128)(2,1)} %bitcast.15, s32[4]{0:T(128)} %len_hbm.1, ...), custom_call_target="tpu_custom_call" | custom-call | tf_op jit(solution)/shard_map/layer/pallas_call | solution.py:578
  61.2 0.6 copy.17
